TPU v7x, 512 devices: a whole 4x8x8 slice. The times are simulated.
512 devices in a mesh: sp: 128 (over z, y, core), tp: 4 (over x).
Axes of the slice: x: 4, y: 8, z: 8, core: 2. Of those that a mesh axis runs over, the one named last changes fastest.
Arguments:
- tokens: bfloat16 [16384, 2048], P(('sp', 'tp')), may hold values from -6 to 6
- doc_lengths: int32 [16], replicated, may hold values from 1 to 10240, 16384 in all
- query_down: bfloat16 [2048, 512], replicated, may hold values from -0.125 to 0.125
- latent_down: bfloat16 [2048, 256], replicated, may hold values from -0.125 to 0.125
- rope_down: bfloat16 [2048, 32], replicated, may hold values from -0.125 to 0.125
- query_latent_gain: float32 [512], replicated, may hold values from 0.1 to 1.9
- latent_gain: float32 [256], replicated, may hold values from 0.1 to 1.9
- query_up: bfloat16 [512, 768], P(None, 'tp'), may hold values from -0.25 to 0.25
- key_up: bfloat16 [256, 512], P(None, 'tp'), may hold values from -0.375 to 0.375
- value_up: bfloat16 [256, 512], P(None, 'tp'), may hold values from -0.375 to 0.375
- query_gain: float32 [96], replicated, may hold values from 0.5 to 15
- key_gain: float32 [96], replicated, may hold values from 0.5 to 15
- output_gain: float32 [512], replicated, may hold values from 0.1 to 1.9
- output_weight: bfloat16 [512, 2048], P(None, 'tp'), may hold values from -0.25 to 0.25
Outputs:
- layer_output: bfloat16 [16384, 2048], P('sp', 'tp')
- log_totals: float32 [8, 16384], P('tp', 'sp')
Inputs may be any that keep to these rules, and one draw needn't show every extreme that they name: `doc_lengths`: the lengths sum to 16384; the longest is exactly 10240.
All inputs are finite; a program needn't handle non-finite values.
Results may differ from a plain program's by a relative error of at most 0.019.
The roundings to bfloat16 on the way count: a program that leaves them out, or rounds other values in their place, can miss the bound.
Values may be sent and summed in bfloat16 or wider, within the bound.
A program may use at most 64 MiB of HBM per device.

v0:
```python
import math

import jax
import jax.numpy as jnp
from jax import lax
from jax.sharding import PartitionSpec as P

NOPE = 64
ROPE = 32
VD = 64


EPS = 1e-06
THETA = 10000.0
NEG = -1e30
key_span = 2048


def from_everyone(value, axis):
    copies = jnp.broadcast_to(value, (lax.axis_size(axis), *value.shape))
    return lax.all_to_all(copies, axis, split_axis=0, concat_axis=0, tiled=True)


def joined_along(blocks, dim):
    blocks = jnp.moveaxis(blocks, 0, dim)
    dims = blocks.shape
    return blocks.reshape(*dims[:dim], dims[dim] * dims[dim + 1], *dims[dim + 2 :])


def gather_directly(value, axis, dim):
    blocks = from_everyone(value, axis)
    return joined_along(blocks, dim)


def in_one_piece(arrays, axis, dim, along):
    widths = [a.shape[along] for a in arrays]
    both = jnp.concatenate(arrays, axis=along)
    filled = gather_directly(both, axis, dim)
    return tuple(jnp.split(filled, [sum(widths[:k]) for k in range(1, len(widths))], axis=along))


def in_one_piece_2(arrays, axis, dim, along):
    both = jnp.concatenate(arrays, axis=along)
    filled, at, done = (lax.all_gather(both, axis, axis=dim, tiled=True), 0, [])
    for a in arrays:
        done.append(lax.slice_in_dim(filled, at, at + a.shape[along], axis=along))
        at += a.shape[along]
    return tuple(done)


def norm_rows(matrix, scaling):
    mean_square = jnp.mean(matrix * matrix, axis=-1, keepdims=True)
    return matrix * lax.rsqrt(mean_square + EPS) * scaling


def rotate(matrix, places):
    half_width = matrix.shape[-1] // 2
    inverse = THETA ** (-jnp.arange(half_width, dtype=jnp.float32) / half_width)
    angles = places.astype(jnp.float32)[:, None, None] * inverse
    cosine = jnp.cos(angles)
    sine_part = jnp.sin(angles)
    leading = matrix[..., :half_width]
    trailing = matrix[..., half_width:]
    return jnp.concatenate(
        [leading * cosine - trailing * sine_part, trailing * cosine + leading * sine_part], axis=-1
    )


def doc_index(places, doc_ends):
    return jnp.sum((places[:, None] >= doc_ends[None, :]).astype(jnp.int32), axis=1)


def head_keys(latent_rows, rope_rows, places, key_up, value_up, key_gain):
    row_count = latent_rows.shape[0]
    head_count = key_up.shape[1] // NOPE
    plain_part = jnp.dot(latent_rows, key_up, preferred_element_type=jnp.float32).reshape(
        row_count, head_count, NOPE
    )
    shared_part = jnp.broadcast_to(
        rope_rows.astype(jnp.float32)[:, None, :], (row_count, head_count, ROPE)
    )
    joined = norm_rows(jnp.concatenate([plain_part, shared_part], axis=-1), key_gain)
    key_block = jnp.concatenate(
        [joined[..., :NOPE], rotate(joined[..., NOPE:], places)], axis=-1
    ).astype(jnp.bfloat16)
    value_block = jnp.dot(latent_rows, value_up, preferred_element_type=jnp.float32).astype(
        jnp.bfloat16
    )
    return (key_block, value_block.reshape(row_count, head_count, VD))


def absorb_block(running, queries, query_docs, key_block, value_block, key_docs, score_scale):
    row_top, row_total, weighted = running
    scores = (
        jnp.einsum("qhd,khd->hqk", queries, key_block, preferred_element_type=jnp.float32)
        * score_scale
    )
    allowed = (query_docs[:, None] == key_docs[None, :])[None]
    scores = jnp.where(allowed, scores, NEG)
    newest_top = jnp.maximum(row_top, jnp.max(scores, axis=-1))
    weights = jnp.where(allowed, jnp.exp(scores - newest_top[..., None]), 0.0)
    rescale = jnp.exp(row_top - newest_top)
    row_total = row_total * rescale + jnp.sum(weights, axis=-1)
    update = jnp.einsum(
        "hqk,khd->qhd",
        weights.astype(jnp.bfloat16),
        value_block,
        preferred_element_type=jnp.float32,
    )
    weighted = weighted * jnp.transpose(rescale)[:, :, None] + update
    return (newest_top, row_total, weighted)


def per_device(
    tokens,
    doc_lengths,
    query_down,
    latent_down,
    rope_down,
    query_latent_gain,
    latent_gain,
    query_up,
    key_up,
    value_up,
    query_gain,
    key_gain,
    output_gain,
    output_weight,
):
    query_latent = norm_rows(
        jnp.dot(tokens, query_down, preferred_element_type=jnp.float32), query_latent_gain
    ).astype(jnp.bfloat16)
    key_latent = norm_rows(
        jnp.dot(tokens, latent_down, preferred_element_type=jnp.float32), latent_gain
    ).astype(jnp.bfloat16)
    rope_key = jnp.dot(tokens, rope_down, preferred_element_type=jnp.float32).astype(jnp.bfloat16)
    query_rows, latent_rows, rope_rows = in_one_piece(
        (query_latent, key_latent, rope_key), "tp", 0, 1
    )
    row_count = query_rows.shape[0]
    head_width = NOPE + ROPE
    head_count = query_up.shape[1] // head_width
    row_offset = lax.axis_index("sp") * row_count
    places = row_offset + jnp.arange(row_count, dtype=jnp.int32)
    doc_ends = jnp.cumsum(doc_lengths)
    query_docs = doc_index(places, doc_ends)
    lowest_doc = query_docs[0]
    highest_doc = query_docs[row_count - 1]
    query_raw = jnp.dot(query_rows, query_up, preferred_element_type=jnp.float32).reshape(
        row_count, head_count, head_width
    )
    query_raw = norm_rows(query_raw, query_gain)
    queries = jnp.concatenate(
        [query_raw[..., :NOPE], rotate(query_raw[..., NOPE:], places)], axis=-1
    ).astype(jnp.bfloat16)
    score_scale = head_width ** (-0.5)
    initial = (
        jnp.full((head_count, row_count), NEG, jnp.float32),
        jnp.zeros((head_count, row_count), jnp.float32),
        jnp.zeros((row_count, head_count, VD), jnp.float32),
    )
    own_keys, own_values = head_keys(latent_rows, rope_rows, places, key_up, value_up, key_gain)

    def from_heads(sliced):
        return (
            sliced[0].reshape(-1, head_count, head_width),
            sliced[1].reshape(-1, head_count, VD),
        )

    pieces = in_one_piece_2(
        (
            own_keys.reshape(row_count, head_count * head_width),
            own_values.reshape(row_count, head_count * VD),
        ),
        "sp",
        0,
        1,
    )
    piece_rows = pieces[0].shape[0]
    span_rows = math.gcd(piece_rows, key_span)

    def one_span(turn_index, carried):
        offset = turn_index * span_rows
        sliced = tuple(
            (lax.dynamic_slice_in_dim(member, offset, span_rows, 0) for member in pieces)
        )
        key_places = offset + jnp.arange(span_rows, dtype=jnp.int32)
        key_docs = doc_index(key_places, doc_ends)
        touches = (key_docs[0] <= highest_doc) & (key_docs[span_rows - 1] >= lowest_doc)

        def absorb_span(current):
            key_block, value_block = from_heads(sliced)
            return absorb_block(
                current, queries, query_docs, key_block, value_block, key_docs, score_scale
            )

        def pass_over(current):
            return current

        return lax.cond(touches, absorb_span, pass_over, carried)

    row_top, row_total, weighted = lax.fori_loop(0, piece_rows // span_rows, one_span, initial)
    head_out = (
        (weighted / jnp.transpose(row_total)[:, :, None])
        .astype(jnp.bfloat16)
        .reshape(row_count, head_count * VD)
    )
    log_totals = row_top + jnp.log(row_total)
    every_head = gather_directly(head_out, "tp", 1)
    normed = norm_rows(every_head.astype(jnp.float32), output_gain).astype(jnp.bfloat16)
    layer_output = jnp.dot(normed, output_weight, preferred_element_type=jnp.float32).astype(
        jnp.bfloat16
    )
    return (layer_output, log_totals)


def solution(mesh):
    return jax.shard_map(
        per_device,
        mesh=mesh,
        in_specs=(
            P(("sp", "tp"), None),
            P(),
            P(),
            P(),
            P(),
            P(),
            P(),
            P(None, "tp"),
            P(None, "tp"),
            P(None, "tp"),
            P(),
            P(),
            P(),
            P(None, "tp"),
        ),
        out_specs=(P("sp", "tp"), P("tp", "sp")),
        check_vma=False,
    )
```

profile of v0, /device:TPU:192, one launch (start us, length us, event | category | flops | bytes accessed | tf_op | source)
XLA Modules:
  0.0 203.6 jit_solution(15016380440380774282)
XLA Ops:
  7.3 1.5 copy-done
  8.8 1.5 multiply_reduce_fusion.3
  10.3 0.4 multiply_reduce_fusion.4
  11.1 0.7 broadcast_in_dim.80
  11.8 4.3 %all-to-all-start = ((bf16[4,32,800]{2,1,0:T(8,128)(2,1)}), bf16[4,32,800]{2,1,0:T(8,128)(2,1)S(1)}, u32[]{:S(2)}, u32[]{:S(2)}) async-start(bf16[4,32,800]{2,1,0:T(8,128)(2,1)} %broadcast_in_dim.80), calls=%async_computation | async-start | bytes 458752 | tf_op jit(solution)/shard_map/all_to_all | solution.py:21
  16.2 6.4 %all-to-all-done = bf16[4,32,800]{2,1,0:T(8,128)(2,1)S(1)} async-done(((bf16[4,32,800]{2,1,0:T(8,128)(2,1)}), bf16[4,32,800]{2,1,0:T(8,128)(2,1)S(1)}, u32[]{:S(2)}, u32[]{:S(2)}) %all-to-all-start) | async-done | bytes 204832 | tf_op jit(solution)/shard_map/all_to_all | solution.py:21
  23.6 0.6 pad_maximum_fusion.1
  24.6 0.7 fusion.21
  25.3 95.9 %all-gather.2.cloned.1.call-done = bf16[16384,320]{0,1:T(8,128)(2,1)} async-done(((bf16[128,320]{0,1:T(8,128)(2,1)}), bf16[16384,320]{0,1:T(8,128)(2,1)}) %all-gather.2.cloned.1.call-update) | async-done | bytes 10485776 | tf_op jit(solution)/shard_map/all_gather | solution.py:44
  121.2 6.0 %slice.67 = bf16[16384,192]{0,1:T(8,128)(2,1)} slice(bf16[16384,320]{0,1:T(8,128)(2,1)} %all-gather.2.cloned.1.call-done), slice={[0:16384], [0:192]} | slice | bytes 12582912 | tf_op jit(solution)/shard_map/slice | solution.py:46
  127.1 4.5 %slice.71 = bf16[16384,128]{0,1:T(8,128)(2,1)} slice(bf16[16384,320]{0,1:T(8,128)(2,1)} %all-gather.2.cloned.1.call-done), slice={[0:16384], [192:320]} | slice | bytes 8388608 | tf_op jit(solution)/shard_map/slice | solution.py:46
  131.7 53.0 %while.17 = (s32[]{:T(128)}, f32[2,128]{1,0:T(2,128)S(1)}, f32[2,128]{1,0:T(2,128)S(1)}, f32[128,2,64]{0,2,1:T(8,128)S(1)}, s32[16]{0:T(128)S(1)}, /*index=5*/s3...) while((s32[]{:T(128)}, f32[2,128]{1,0:T(2,128)S(1)}, ...), condition=%wide.region_12.13_spmd, body=%wide.region_6.12_spmd.sunk | while | flops 172884736 | bytes 11502497 | solution.py:202
  131.8 0.6 fusion.37
  135.1 0.6 fusion.37
  138.2 4.5 %conditional.2 = ((f32[2,128]{1,0:T(2,128)S(1)}, f32[2,128]{1,0:T(2,128)S(1)}, f32[128,2,64]{0,2,1:T(8,128)S(1)})) conditional(s32[]{:T(128)} %convert_element_type.108, (f32[2,128]{1,0:T(2,128)S(1)}, f32[2,128]{1,0:T(2,128)S(1)}, f32[128,2,64]{0,2,1:T(8,128)S(1)}) %tuple.62, (s32[128]{0:T(128)S(1)}, s32[2048]{0:T(1024)S(1)}, s32[]{:T(128)}, ...), branch_computations={%region_8.8_spmd, %region_9.11_spmd} | conditional | flops 172786432 | bytes 11477578 | solution.py:200
  138.2 1.2 constant_dynamic-slice_fusion.1
  139.8 0.7 fusion.19
  140.5 1.1 constant_dynamic-slice_fusion
  141.5 0.7 fusion.4
  142.2 0.4 fusion.3
  142.8 0.6 fusion.37
  145.9 4.5 %conditional.2 = ((f32[2,128]{1,0:T(2,128)S(1)}, f32[2,128]{1,0:T(2,128)S(1)}, f32[128,2,64]{0,2,1:T(8,128)S(1)})) conditional(s32[]{:T(128)} %convert_element_type.108, (f32[2,128]{1,0:T(2,128)S(1)}, f32[2,128]{1,0:T(2,128)S(1)}, f32[128,2,64]{0,2,1:T(8,128)S(1)}) %tuple.62, (s32[128]{0:T(128)S(1)}, s32[2048]{0:T(1024)S(1)}, s32[]{:T(128)}, ...), branch_computations={%region_8.8_spmd, %region_9.11_spmd} | conditional | flops 172786432 | bytes 11477578 | solution.py:200
  146.0 1.2 constant_dynamic-slice_fusion.1
  147.2 0.3 broadcast_compare_fusion
  147.5 0.7 fusion.19
  148.2 1.1 constant_dynamic-slice_fusion
  149.3 0.7 fusion.4
  150.0 0.4 fusion.3
  150.6 0.6 fusion.37
  153.7 4.5 %conditional.2 = ((f32[2,128]{1,0:T(2,128)S(1)}, f32[2,128]{1,0:T(2,128)S(1)}, f32[128,2,64]{0,2,1:T(8,128)S(1)})) conditional(s32[]{:T(128)} %convert_element_type.108, (f32[2,128]{1,0:T(2,128)S(1)}, f32[2,128]{1,0:T(2,128)S(1)}, f32[128,2,64]{0,2,1:T(8,128)S(1)}) %tuple.62, (s32[128]{0:T(128)S(1)}, s32[2048]{0:T(1024)S(1)}, s32[]{:T(128)}, ...), branch_computations={%region_8.8_spmd, %region_9.11_spmd} | conditional | flops 172786432 | bytes 11477578 | solution.py:200
  153.7 1.2 constant_dynamic-slice_fusion.1
  155.3 0.7 fusion.19
  155.9 1.1 constant_dynamic-slice_fusion
  157.0 0.7 fusion.4
  157.7 0.4 fusion.3
  158.3 0.6 fusion.37
  161.4 4.5 %conditional.2 = ((f32[2,128]{1,0:T(2,128)S(1)}, f32[2,128]{1,0:T(2,128)S(1)}, f32[128,2,64]{0,2,1:T(8,128)S(1)})) conditional(s32[]{:T(128)} %convert_element_type.108, (f32[2,128]{1,0:T(2,128)S(1)}, f32[2,128]{1,0:T(2,128)S(1)}, f32[128,2,64]{0,2,1:T(8,128)S(1)}) %tuple.62, (s32[128]{0:T(128)S(1)}, s32[2048]{0:T(1024)S(1)}, s32[]{:T(128)}, ...), branch_computations={%region_8.8_spmd, %region_9.11_spmd} | conditional | flops 172786432 | bytes 11477578 | solution.py:200
  161.4 1.2 constant_dynamic-slice_fusion.1
  162.7 0.3 broadcast_compare_fusion
  163.0 0.7 fusion.19
  163.7 1.1 constant_dynamic-slice_fusion
  164.8 0.7 fusion.4
  165.4 0.4 fusion.3
  166.0 0.6 fusion.37
  169.2 4.5 %conditional.2 = ((f32[2,128]{1,0:T(2,128)S(1)}, f32[2,128]{1,0:T(2,128)S(1)}, f32[128,2,64]{0,2,1:T(8,128)S(1)})) conditional(s32[]{:T(128)} %convert_element_type.108, (f32[2,128]{1,0:T(2,128)S(1)}, f32[2,128]{1,0:T(2,128)S(1)}, f32[128,2,64]{0,2,1:T(8,128)S(1)}) %tuple.62, (s32[128]{0:T(128)S(1)}, s32[2048]{0:T(1024)S(1)}, s32[]{:T(128)}, ...), branch_computations={%region_8.8_spmd, %region_9.11_spmd} | conditional | flops 172786432 | bytes 11477578 | solution.py:200
  169.2 1.2 constant_dynamic-slice_fusion.1
  170.4 0.3 broadcast_compare_fusion
  170.7 0.7 fusion.19
  171.4 1.1 constant_dynamic-slice_fusion
  172.5 0.7 fusion.4
  173.2 0.4 fusion.3
  173.8 0.6 fusion.37
  176.9 4.5 %conditional.2 = ((f32[2,128]{1,0:T(2,128)S(1)}, f32[2,128]{1,0:T(2,128)S(1)}, f32[128,2,64]{0,2,1:T(8,128)S(1)})) conditional(s32[]{:T(128)} %convert_element_type.108, (f32[2,128]{1,0:T(2,128)S(1)}, f32[2,128]{1,0:T(2,128)S(1)}, f32[128,2,64]{0,2,1:T(8,128)S(1)}) %tuple.62, (s32[128]{0:T(128)S(1)}, s32[2048]{0:T(1024)S(1)}, s32[]{:T(128)}, ...), branch_computations={%region_8.8_spmd, %region_9.11_spmd} | conditional | flops 172786432 | bytes 11477578 | solution.py:200
  176.9 1.2 constant_dynamic-slice_fusion.1
  178.5 0.7 fusion.19
  179.1 1.1 constant_dynamic-slice_fusion
  180.2 0.7 fusion.4
  180.9 0.4 fusion.3
  181.5 0.6 fusion.37
  184.7 0.7 broadcast_in_dim.82
  185.4 4.2 %all-to-all-start.1 = ((bf16[4,128,128]{1,2,0:T(8,128)(2,1)}), bf16[4,128,128]{1,2,0:T(8,128)(2,1)S(1)}, u32[]{:S(2)}, u32[]{:S(2)}) async-start(bf16[4,128,128]{1,2,0:T(8,128)(2,1)} %broadcast_in_dim.82), calls=%async_computation.1 | async-start | bytes 262144 | tf_op jit(solution)/shard_map/all_to_all | solution.py:21
  189.6 0.6 log_add_fusion
  190.2 5.4 %all-to-all-done.1 = bf16[4,128,128]{1,2,0:T(8,128)(2,1)S(1)} async-done(((bf16[4,128,128]{1,2,0:T(8,128)(2,1)}), bf16[4,128,128]{1,2,0:T(8,128)(2,1)S(1)}, u32[]{:S(2)}, u32[]{:S(2)}) %all-to-all-start.1) | async-done | bytes 131104 | tf_op jit(solution)/shard_map/all_to_all | solution.py:21
  195.8 0.9 convolution_convert_fusion
  (105 shorter events, 4.1 us)
Async XLA Ops:
  7.2 1.6 copy-start
  7.2 3.1 %copy-start.1 = (bf16[32,2048]{1,0:T(8,128)(2,1)S(1)}, bf16[32,2048]{1,0:T(8,128)(2,1)}, u32[]{:S(2)}) copy-start(bf16[32,2048]{1,0:T(8,128)(2,1)} %param.18) | copy-start | bytes 393220
  7.2 3.1 %copy-start.2 = (bf16[2048,256]{1,0:T(8,128)(2,1)S(1)}, bf16[2048,256]{1,0:T(8,128)(2,1)}, u32[]{:S(2)}) copy-start(bf16[2048,256]{1,0:T(8,128)(2,1)} %param.21) | copy-start | bytes 3145732
  7.2 3.5 %copy-start.5 = (bf16[2048,32]{0,1:T(8,128)(2,1)S(1)}, bf16[2048,32]{0,1:T(8,128)(2,1)}, u32[]{:S(2)}) copy-start(bf16[2048,32]{0,1:T(8,128)(2,1)} %param.22) | copy-start | bytes 393220
  7.2 3.7 %copy-start.9 = (f32[512]{0:T(512)S(1)}, f32[512]{0:T(512)}, u32[]{:S(2)}) copy-start(f32[512]{0:T(512)} %param.23) | copy-start | bytes 6148
  7.2 3.8 %copy-start.10 = (f32[256]{0:T(256)S(1)}, f32[256]{0:T(256)}, u32[]{:S(2)}) copy-start(f32[256]{0:T(256)} %param.24) | copy-start | bytes 3076
  7.2 15.4 %copy-start.6 = (bf16[256,128]{1,0:T(8,128)(2,1)S(1)}, bf16[256,128]{1,0:T(8,128)(2,1)}, u32[]{:S(2)}) copy-start(bf16[256,128]{1,0:T(8,128)(2,1)} %param.26) | copy-start | bytes 196612
  7.2 15.7 %copy-start.4 = (bf16[512,192]{0,1:T(8,128)(2,1)S(1)}, bf16[512,192]{0,1:T(8,128)(2,1)}, u32[]{:S(2)}) copy-start(bf16[512,192]{0,1:T(8,128)(2,1)} %param.25) | copy-start | bytes 589828
  10.2 13.0 %copy-start.11 = (f32[96]{0:T(128)S(1)}, f32[96]{0:T(128)}, u32[]{:S(2)}) copy-start(f32[96]{0:T(128)} %param.28) | copy-start | bytes 1156
  10.3 13.0 %copy-start.12 = (f32[96]{0:T(128)S(1)}, f32[96]{0:T(128)}, u32[]{:S(2)}) copy-start(f32[96]{0:T(128)} %param.29) | copy-start | bytes 1156
  10.3 13.1 %copy-start.7 = (bf16[256,128]{1,0:T(8,128)(2,1)S(1)}, bf16[256,128]{1,0:T(8,128)(2,1)}, u32[]{:S(2)}) copy-start(bf16[256,128]{1,0:T(8,128)(2,1)} %param.27) | copy-start | bytes 196612
  10.3 14.0 %copy-start.13 = (s32[16]{0:T(128)S(1)}, s32[16]{0:T(128)}, u32[]{:S(2)}) copy-start(s32[16]{0:T(128)} %param.19) | copy-start | bytes 196
  11.8 10.8 %all-to-all-start = ((bf16[4,32,800]{2,1,0:T(8,128)(2,1)}), bf16[4,32,800]{2,1,0:T(8,128)(2,1)S(1)}, u32[]{:S(2)}, u32[]{:S(2)}) async-start(bf16[4,32,800]{2,1,0:T(8,128)(2,1)} %broadcast_in_dim.80), calls=%async_computation | async-start | bytes 458752 | tf_op jit(solution)/shard_map/all_to_all | solution.py:21
  16.1 105.1 %all-gather.2.cloned.1.call-start = ((), (), s32[]{:S(2)}) async-start(), calls=%async_computation.2 | async-start | bytes 10567680 | tf_op jit(solution)/shard_map/all_gather | solution.py:44
  131.7 64.0 %copy-start.8 = (f32[512]{0:T(512)S(1)}, f32[512]{0:T(512)}, u32[]{:S(2)}) copy-start(f32[512]{0:T(512)} %param.30) | copy-start | bytes 6148
  131.7 64.2 %copy-start.3 = (bf16[512,512]{1,0:T(8,128)(2,1)S(1)}, bf16[512,512]{1,0:T(8,128)(2,1)}, u32[]{:S(2)}) copy-start(bf16[512,512]{1,0:T(8,128)(2,1)} %param.31) | copy-start | bytes 1572868
  185.4 10.2 %all-to-all-start.1 = ((bf16[4,128,128]{1,2,0:T(8,128)(2,1)}), bf16[4,128,128]{1,2,0:T(8,128)(2,1)S(1)}, u32[]{:S(2)}, u32[]{:S(2)}) async-start(bf16[4,128,128]{1,2,0:T(8,128)(2,1)} %broadcast_in_dim.82), calls=%async_computation.1 | async-start | bytes 262144 | tf_op jit(solution)/shard_map/all_to_all | solution.py:21
Sparse Core Ops, SparseCore 0:
  24.4 96.7 all-gather.1
where the time goes:
time: 204 us
  waiting for transfers between devices  108 us (53%)
  local copies, waits for them, and re-layouts  32.9 us (16%)
  loops' own time  20.8 us (10%)
  between operations  14.4 us (7%)
  matrix products  11.6 us (6%)
  starting transfers between devices  8.54 us (4%)
  other arithmetic  7.76 us (4%)
    all_gather x1, waiting for transfers between devices, in_one_piece_2(): filled, at, done = (lax.all_gather(both, axis, axis=dim, tiled=True), 0, [])  95.9 us
    another operation x1, loops' own time, per_device(): lax.fori_loop(0, piece_rows // span_rows, one_span, initial)  20.4 us
    dynamic_slice x12, local copies, waits for them, and re-layouts, one_span(): lax.dynamic_slice_in_dim(member, offset, span_rows, 0)  13.7 us
    all_to_all x2, waiting for transfers between devices, from_everyone(): return lax.all_to_all(copies, axis, split_axis=0, concat_axis=0, tiled=True)  11.8 us
    slice x2, local copies, waits for them, and re-layouts, in_one_piece_2(): done.append(lax.slice_in_dim(filled, at, at + a.shape[along], axis=along))  10.5 us
    all_to_all x2, starting transfers between devices, from_everyone(): return lax.all_to_all(copies, axis, split_axis=0, concat_axis=0, tiled=True)  8.54 us
    slice x8, local copies, waits for them, and re-layouts, one_span(): key_docs[span_rows - 1] >= lowest_doc  4.88 us
    dot_general x6, matrix products, absorb_block(): jnp.einsum('hqk,khd->qhd', weights.astype(jnp.bfloat16), value_block, pre...  4.1 us
  transfers between devices with their start and end apart: 3, of which 3 were waited for; matrix products, arithmetic and copies ran while one was open for 1% of the time, Pallas kernels for 0%

commit v1 on v0

v1 whole, which is shorter than its diff:
```python
import functools

import jax
import jax.numpy as jnp
import numpy as np
from jax import lax
from jax.experimental import pallas as pl
from jax.experimental.pallas import tpu as pltpu
from jax.sharding import PartitionSpec as P

NOPE = 64
ROPE = 32
VD = 64
NDOC = 16
WIDTH = NOPE + ROPE
EPS = 1e-06
THETA = 10000.0
APART = -float(2**20)
SCALE = WIDTH**-0.5
LOG2E = 1.4426950408889634
F32 = jnp.float32
BF16 = jnp.bfloat16
MESH = pl.DeviceIdType.MESH
DOC_LANE = 64


def split_of(count):
    return {128: (8, 8, 2), 8: (2, 2, 2), 16: (2, 4, 2)}[count]


def tables(blocks):
    half = ROPE // 2
    inverse = THETA ** (-(np.arange(128) % half).astype(np.float64) / half)
    fine = np.arange(128)[:, None] * inverse[None]
    coarse = (np.arange(blocks) * 128)[:, None] * inverse[None]
    fine = np.stack([np.cos(fine), np.sin(fine)]).astype(np.float32)
    coarse = np.stack([np.cos(coarse), np.sin(coarse)]).astype(np.float32)
    return fine, coarse


def query_columns():
    out = np.zeros((2 * WIDTH, 384), np.float32)
    for j in range(128):
        out[(j // 64) * WIDTH + j % 64, j] = 1
        head, entry = (j % 64) // 32, j % 32
        out[head * WIDTH + NOPE + entry, 128 + j] = 1
        out[head * WIDTH + NOPE + (entry + 16) % 32, 256 + j] = 1
    return out


def rope_spread():
    out = np.zeros((128, 1024), np.float32)
    for g in range(4):
        for j in range(64):
            out[32 * g + j % 32, 256 * g + j] = 1
            out[32 * g + (j % 32 + 16) % 32, 256 * g + 128 + j] = 1
    return out


def sum_matrix(rope_lanes):
    out = np.zeros((256, 256), np.float32)
    for col in range(256):
        head = col // 64 if col < 128 else ((col - 128) // 32) % 2
        for i in range(128):
            out[i, col] = i // 64 == head
        for i in range(64):
            if rope_lanes == 32:
                out[128 + i, col] = i < 32
            else:
                out[128 + i, col] = i // 32 == head
    return out


def dot(a, b):
    return jnp.dot(a, b, preferred_element_type=F32)


def dot_t(a, b):
    return lax.dot_general(a, b, (((1,), (1,)), ((), ())), preferred_element_type=F32)


def lanes(rows, width=128):
    return lax.broadcasted_iota(jnp.int32, (rows, width), 1)


def rows_of(rows, width=128):
    return lax.broadcasted_iota(jnp.int32, (rows, width), 0)


def head_sums(squares, matrix):
    high = squares.astype(BF16)
    low = (squares - high.astype(F32)).astype(BF16)
    return dot(high, matrix) + dot(low, matrix)


def kernel(
    Z, Y, C, X,
    tok, doclen, qdown, ldown, rdown, qlgain, lgain, qup, kup, vup, gains, ogain, oweight,
    fine, coarse, qcols, spread, ksum, qsum,
    out, logs,
    qlbuf, klbuf, rkbuf, qbuf, kall, vtall, sbuf, pbuf, vupt, osend, lsend, orecv, lrecv, hobuf, bounds,
    ql_s, ql_r, kz_s, kz_r, kx_s, kx_r, kc_s, kc_r, qy_s, qy_r, o_s, o_r, ho_s, ho_r,
):
    s = lax.axis_index("sp")
    t = lax.axis_index("tp")
    z = s // (Y * C)
    y = lax.rem(s // C, Y)
    c = lax.rem(s, C)
    gz = Z * 32

    def at(zz, yy, cc):
        return (zz * Y + yy) * C + cc

    def zpeer(k):
        zz = lax.rem(z + k, Z)
        return zz, (at(zz, y, c), t)

    def ypeer(k):
        yy = lax.rem(y + k, Y)
        return yy, (at(z, yy, c), t)

    def xpeer(k):
        xx = lax.rem(t + k, X)
        return xx, (s, xx)

    other = (at(z, y, 1 - c), t)

    def remote(src, dst, ss, rs, who):
        return pltpu.make_async_remote_copy(
            src_ref=src, dst_ref=dst, send_sem=ss, recv_sem=rs, device_id=who, device_id_type=MESH
        )

    barrier = pltpu.get_barrier_semaphore()
    peers = [zpeer(k)[1] for k in range(1, Z)] + [ypeer(k)[1] for k in range(1, Y)]
    peers += [xpeer(k)[1] for k in range(1, X)] + [other]
    for who in peers:
        pl.semaphore_signal(barrier, inc=1, device_id=who, device_id_type=MESH)

    x = tok[...]
    qd = dot(x, qdown[...])
    qd = qd * lax.rsqrt(jnp.mean(qd * qd, axis=-1, keepdims=True) + EPS) * qlgain[...]
    qlbuf[t] = qd.astype(BF16)
    kd = dot(x, ldown[...])
    kd = kd * lax.rsqrt(jnp.mean(kd * kd, axis=-1, keepdims=True) + EPS) * lgain[...]
    klbuf[c, t, z] = kd.astype(BF16)
    rk = dot(x, rdown[...]).astype(BF16)
    four = (lanes(32) % 32 == rows_of(32)).astype(F32).astype(BF16)
    rk4 = dot(rk, four)
    group = lanes(8) // 32
    packed = jnp.where(group == 0, rk4[0:8], jnp.where(group == 1, rk4[8:16], jnp.where(group == 2, rk4[16:24], rk4[24:32])))
    rkbuf[c, t, z] = packed

    pl.semaphore_wait(barrier, len(peers))

    sends = []
    for k in range(1, X):
        _, who = xpeer(k)
        copy = remote(qlbuf.at[t], qlbuf.at[t], ql_s.at[k], ql_r.at[k], who)
        copy.start()
        sends.append(copy)
    for k in range(1, Z):
        _, who = zpeer(k)
        for n, buf in enumerate((klbuf, rkbuf)):
            copy = remote(buf.at[c, t, z], buf.at[c, t, z], kz_s.at[n, k], kz_r.at[n, k], who)
            copy.start()
            sends.append(copy)

    lane1 = lanes(1)
    starts = jnp.full((1, 128), 1 << 30, jnp.int32)
    ends = jnp.zeros((1, 128), jnp.int32)
    total = jnp.int32(0)
    for d in range(NDOC):
        starts = jnp.where(lane1 == DOC_LANE + d, total, starts)
        total = total + doclen[d]
        ends = jnp.where(lane1 == DOC_LANE + d, total, ends)
    bounds[0:1, :] = starts
    bounds[1:2, :] = ends
    qweight = dot(qup[...], qcols[...]).astype(BF16)
    vupt[...] = jnp.transpose(vup[...].astype(F32)).astype(BF16)

    def turn(block, first, count):
        cb = coarse[0, pl.ds(block, 1), :]
        sb = coarse[1, pl.ds(block, 1), :]
        cf = fine[0, pl.ds(first, count), :]
        sf = fine[1, pl.ds(first, count), :]
        return cb * cf - sb * sf, sb * cf + cb * sf

    for k in range(1, X):
        xx = lax.rem(t - k + X, X)
        remote(qlbuf.at[xx], qlbuf.at[xx], ql_s.at[k], ql_r.at[k], (s, xx)).wait_recv()
    ql = qlbuf[...].reshape(128, qlbuf.shape[2])
    qq = dot(ql, qweight)
    q0, q1, q2 = qq[:, 0:128], qq[:, 128:256], qq[:, 256:384]
    qs = head_sums(jnp.concatenate([q0 * q0, q1 * q1], axis=1), qsum[...])
    qs = lax.rsqrt(qs * (1.0 / WIDTH) + EPS)
    cosine, sine = turn(s, 0, 128)
    plain = q0 * qs[:, 0:128] * gains[0:1, :]
    rope = (q1 * gains[1:2, :] * cosine + q2 * gains[2:3, :] * sine) * qs[:, 128:256]
    qbuf[y, 0:128, :] = plain.astype(BF16)
    qbuf[y, 128:192, :] = jnp.where(lanes(64) < 64, rope[0:64], rope[64:128]).astype(BF16)
    for k in range(1, Y):
        _, who = ypeer(k)
        copy = remote(qbuf.at[y], qbuf.at[y], qy_s.at[k], qy_r.at[k], who)
        copy.start()
        sends.append(copy)

    for k in range(1, Z):
        zz = lax.rem(z - k + Z, Z)
        for n, buf in enumerate((klbuf, rkbuf)):
            slot = buf.at[c, t, zz]
            remote(slot, slot, kz_s.at[n, k], kz_r.at[n, k], (at(zz, y, c), t)).wait_recv()
    for k in range(1, X):
        _, who = xpeer(k)
        for n, buf in enumerate((klbuf, rkbuf)):
            copy = remote(buf.at[c, t], buf.at[c, t], kx_s.at[n, k], kx_r.at[n, k], who)
            copy.start()
            sends.append(copy)

    def to_core(k):
        xx = lax.rem(t - k + X, X)
        for n, buf in enumerate((klbuf, rkbuf)):
            slot = buf.at[c, xx]
            copy = remote(slot, slot, kc_s.at[n, k], kc_r.at[n, k], other)
            copy.start()
            sends.append(copy)

    def expand(cc, xx):
        kl = klbuf[cc, xx].reshape(gz, klbuf.shape[4])
        index = cc * X + xx
        vtall[index] = dot_t(vupt[...], kl).astype(BF16)
        raw = dot(kl, kup[...])
        spreaded = dot(rkbuf[cc, xx].reshape(Z * 8, 128).astype(BF16), spread[...])

        def rows_from(shift):
            return jnp.concatenate(
                [spreaded[8 * zz : 8 * zz + 8, 256 * g + shift : 256 * g + shift + 128] for zz in range(Z) for g in range(4)],
                axis=0,
            )

        r1, r2 = rows_from(0), rows_from(128)
        sums = head_sums(jnp.concatenate([raw * raw, r1 * r1], axis=1), ksum[...])
        sums = lax.rsqrt(sums * (1.0 / WIDTH) + EPS)
        kall[index, :, 0:128] = (raw * sums[:, 0:128] * gains[3:4, :]).astype(BF16)
        first = pl.multiple_of(xx * 32, 32)
        for zz in range(Z):
            block = at(zz, y, cc)
            cosine, sine = turn(block, first, 32)
            part = slice(zz * 32, zz * 32 + 32)
            turned = (r1[part] * gains[4:5, :] * cosine + r2[part] * gains[5:6, :] * sine) * sums[part, 128:256]
            place = block * 128 + first + rows_of(32)
            inside = (place >= bounds[0:1, :]) & (place < bounds[1:2, :])
            kall[index, part, 128:256] = jnp.where(inside, 1.0, turned).astype(BF16)

    to_core(0)
    expand(c, t)
    for k in range(1, X):
        xx = lax.rem(t - k + X, X)
        for n, buf in enumerate((klbuf, rkbuf)):
            slot = buf.at[c, xx]
            remote(slot, slot, kx_s.at[n, k], kx_r.at[n, k], (s, xx)).wait_recv()
        to_core(k)
        expand(c, xx)
    for k in range(X):
        xx = lax.rem(t - k + X, X)
        for n, buf in enumerate((klbuf, rkbuf)):
            slot = buf.at[1 - c, xx]
            remote(slot, slot, kc_s.at[n, k], kc_r.at[n, k], other).wait_recv()
        expand(1 - c, xx)

    groups = C * X

    def attend(yy):
        block = at(z, yy, c)
        qplain = qbuf[yy, 0:128, :].astype(F32)
        qrope = qbuf[yy, 128:192, :].astype(F32)
        qrope = jnp.concatenate([qrope, pltpu.roll(qrope, 64, 1)], axis=0)
        place = block * 128 + rows_of(128)
        inside = (place >= bounds[0:1, :]) & (place < bounds[1:2, :])
        lane = lanes(128)
        apart = jnp.where((lane >= DOC_LANE) & (lane < DOC_LANE + NDOC) & jnp.logical_not(inside), APART, 0.0)
        both = []
        for h in range(2):
            left = jnp.where(lane // 64 == h, qplain, 0.0)
            right = jnp.where(lane // 32 == h, qrope, apart)
            both.append(jnp.concatenate([left, right], axis=1))
        queries = jnp.concatenate(both, axis=0).astype(BF16)
        top = None
        for g in range(groups):
            scores = dot_t(kall[g], queries)
            sbuf[g] = scores
            most = jnp.max(scores, axis=0, keepdims=True)
            top = most if top is None else jnp.maximum(top, most)
        count = None
        acc = None
        for g in range(groups):
            weights = jnp.exp2((sbuf[g] - top) * (SCALE * LOG2E))
            added = jnp.sum(weights, axis=0, keepdims=True)
            count = added if count is None else count + added
            update = dot(vtall[g], weights.astype(BF16))
            acc = update if acc is None else acc + update
        log = top * SCALE + jnp.log(count)
        lsend[yy] = jnp.where(rows_of(8) == 0, log[:, 0:128], log[:, 128:256])
        inv = 1.0 / count
        osend[yy, 0:64, :] = (acc[0:64, 0:128] * inv[:, 0:128]).astype(BF16)
        osend[yy, 64:128, :] = (acc[64:128, 128:256] * inv[:, 128:256]).astype(BF16)

    def step(i, carry):
        off = jnp.where(lax.rem(i, 2) == 1, (i + 1) // 2, Y - i // 2)
        k = lax.rem(off, Y)
        yy, who = ypeer(k)
        back = lax.rem(Y - k, Y)

        @pl.when(i > 0)
        def _():
            remote(qbuf.at[yy], qbuf.at[yy], qy_s.at[back], qy_r.at[back], who).wait_recv()

        attend(yy)

        @pl.when(i > 0)
        def _():
            remote(osend.at[yy], orecv.at[y], o_s.at[0, k], o_r.at[0, k], who).start()
            remote(lsend.at[yy], lrecv.at[y], o_s.at[1, k], o_r.at[1, k], who).start()

        return carry

    lax.fori_loop(0, Y, step, 0)

    orecv[y] = osend[y]
    lrecv[y] = lsend[y]
    for k in range(1, Y):
        yy = lax.rem(y - k + Y, Y)
        who = (at(z, yy, c), t)
        remote(osend.at[yy], orecv.at[yy], o_s.at[0, k], o_r.at[0, k], who).wait_recv()
        remote(lsend.at[yy], lrecv.at[yy], o_s.at[1, k], o_r.at[1, k], who).wait_recv()
    top = lrecv[0]
    for i in range(1, Y):
        top = jnp.maximum(top, lrecv[i])
    whole = jnp.zeros_like(top)
    acc0 = jnp.zeros((64, 128), F32)
    acc1 = jnp.zeros((64, 128), F32)
    for i in range(Y):
        weight = jnp.exp(lrecv[i] - top)
        whole = whole + weight
        acc0 = acc0 + weight[0:1] * orecv[i, 0:64, :].astype(F32)
        acc1 = acc1 + weight[1:2] * orecv[i, 64:128, :].astype(F32)
    logs[...] = (top + jnp.log(whole))[0:2]
    inv = 1.0 / whole
    heads = jnp.concatenate([acc0 * inv[0:1], acc1 * inv[1:2]], axis=0)
    hobuf[t] = jnp.transpose(heads).astype(BF16)
    for k in range(1, X):
        _, who = xpeer(k)
        copy = remote(hobuf.at[t], hobuf.at[t], ho_s.at[k], ho_r.at[k], who)
        copy.start()
        sends.append(copy)
    for k in range(1, Y):
        yy, who = ypeer(k)
        remote(osend.at[yy], orecv.at[y], o_s.at[0, k], o_r.at[0, k], who).wait_send()
        remote(lsend.at[yy], lrecv.at[y], o_s.at[1, k], o_r.at[1, k], who).wait_send()
    for k in range(1, X):
        xx = lax.rem(t - k + X, X)
        remote(hobuf.at[xx], hobuf.at[xx], ho_s.at[k], ho_r.at[k], (s, xx)).wait_recv()
    full = jnp.concatenate([hobuf[i].astype(F32) for i in range(X)], axis=1)
    normed = full * lax.rsqrt(jnp.mean(full * full, axis=-1, keepdims=True) + EPS) * ogain[...]
    out[...] = dot(normed.astype(BF16), oweight[...]).astype(BF16)
    for copy in sends:
        copy.wait_send()


def gain_rows(gain):
    plain = gain[:NOPE]
    a, b = gain[NOPE : NOPE + 16], gain[NOPE + 16 :]
    rope = jnp.concatenate([a, b])
    swapped = jnp.concatenate([-b, a])
    return [jnp.concatenate([plain] * 2), jnp.concatenate([rope] * 4), jnp.concatenate([swapped] * 4)]


def per_device(
    split, X,
    tokens, doc_lengths, query_down, latent_down, rope_down, query_latent_gain, latent_gain,
    query_up, key_up, value_up, query_gain, key_gain, output_gain, output_weight,
):
    Z, Y, C = split
    blocks = Z * Y * C
    rows = gain_rows(query_gain) + gain_rows(key_gain)
    gains = jnp.stack(rows + [jnp.zeros((128,), F32)] * 2)
    fine, coarse = tables(blocks)
    vm = pl.BlockSpec(memory_space=pltpu.VMEM)
    sm = pl.BlockSpec(memory_space=pltpu.SMEM)
    dma = pltpu.SemaphoreType.DMA
    gz = Z * 32
    groups = C * X
    QR, KVR = query_down.shape[1], latent_down.shape[1]
    const = lambda a: jnp.asarray(a, BF16)
    return pl.pallas_call(
        functools.partial(kernel, Z, Y, C, X),
        out_shape=(
            jax.ShapeDtypeStruct((128, output_weight.shape[1]), BF16),
            jax.ShapeDtypeStruct((2, 128), F32),
        ),
        in_specs=[vm, sm] + [vm] * 17,
        out_specs=(vm, vm),
        scratch_shapes=[
            pltpu.VMEM((X, 32, QR), BF16),
            pltpu.VMEM((C, X, Z, 32, KVR), BF16),
            pltpu.VMEM((C, X, Z, 8, 128), F32),
            pltpu.VMEM((Y, 192, 128), BF16),
            pltpu.VMEM((groups, gz, 256), BF16),
            pltpu.VMEM((groups, 128, gz), BF16),
            pltpu.VMEM((groups, gz, 256), F32),
            pltpu.VMEM((8, 128), F32),
            pltpu.VMEM((128, KVR), BF16),
            pltpu.VMEM((Y, 128, 128), BF16),
            pltpu.VMEM((Y, 8, 128), F32),
            pltpu.VMEM((Y, 128, 128), BF16),
            pltpu.VMEM((Y, 8, 128), F32),
            pltpu.VMEM((X, 128, 128), BF16),
            pltpu.VMEM((8, 128), jnp.int32),
            dma((X,)), dma((X,)),
            dma((2, Z)), dma((2, Z)),
            dma((2, X)), dma((2, X)),
            dma((2, X)), dma((2, X)),
            dma((Y,)), dma((Y,)),
            dma((2, Y)), dma((2, Y)),
            dma((X,)), dma((X,)),
        ],
        compiler_params=pltpu.CompilerParams(
            collective_id=0, has_side_effects=True, vmem_limit_bytes=48 * 2**20
        ),
    )(
        tokens, doc_lengths, query_down, latent_down, rope_down,
        query_latent_gain.reshape(1, -1), latent_gain.reshape(1, -1),
        query_up, key_up, value_up, gains, output_gain.reshape(1, -1), output_weight,
        jnp.asarray(fine), jnp.asarray(coarse), const(query_columns()), const(rope_spread()),
        const(sum_matrix(32)), const(sum_matrix(64)),
    )


def solution(mesh):
    split = split_of(mesh.shape["sp"])
    return jax.shard_map(
        functools.partial(per_device, split, mesh.shape["tp"]),
        mesh=mesh,
        in_specs=(
            P(("sp", "tp"), None),
            P(), P(), P(), P(), P(), P(),
            P(None, "tp"), P(None, "tp"), P(None, "tp"),
            P(), P(), P(),
            P(None, "tp"),
        ),
        out_specs=(P("sp", "tp"), P("tp", "sp")),
        check_vma=False,
    )
```

time: 204 us -> 77.6 us (0.38)
  the two profiles are of different devices: /device:TPU:192 before, /device:TPU:8 now
where the time goes in v1:
time: 77.6 us; the launch traced here: 76.9 us
  Pallas kernels  53.3 us (69%)
  local copies, waits for them, and re-layouts  19.7 us (25%)
  other arithmetic  3.22 us (4%)
    pallas_call x1, Pallas kernels, per_device(): pl.pallas_call(functools.partial(kernel, Z, Y, C, X), out_shape=(jax.Shap...  53.3 us
    unnamed x36, local copies, waits for them, and re-layouts  18.1 us
    another operation x2, other arithmetic, per_device(): gains = jnp.stack(rows + [jnp.zeros((128,), F32)] * 2)  1.61 us
    slice x2, other arithmetic, gain_rows(): a, b = (gain[NOPE:NOPE + 16], gain[NOPE + 16:])  1.61 us

profile of v1, /device:TPU:8, one launch (start us, length us, event | category | flops | bytes accessed | tf_op | source)
XLA Modules:
  0.0 76.9 jit_solution(6523998485940676117)
XLA Ops:
  0.6 0.7 slice.31
  1.4 0.7 slice.35
  2.1 0.8 %maximum_bitcast_fusion.2 = (f32[1,128]{1,0:T(1,128)S(1)}, f32[1,128]{1,0:T(1,128)S(1)}) fusion(f32[64]{0:T(128)} %bitcast.19, f32[32]{0:T(128)S(1)} %slice.35), kind=kLoop, calls=%fused_computation.2 | loop fusion | flops 512 | bytes 1408 | tf_op jit(solution)/shard_map/stack | solution.py:385
  2.9 0.8 %maximum_bitcast_fusion = (f32[1,128]{1,0:T(1,128)S(1)}, f32[1,128]{1,0:T(1,128)S(1)}) fusion(f32[64]{0:T(128)} %bitcast.18, f32[32]{0:T(128)S(1)} %slice.31), kind=kLoop, calls=%fused_computation | loop fusion | flops 512 | bytes 1408 | tf_op jit(solution)/shard_map/stack | solution.py:385
  3.7 0.8 %fusion.1 = (f32[16]{0:T(128)S(1)}, f32[16]{0:T(128)S(1)}) fusion(f32[96]{0:T(128)} %param.30), kind=kLoop, calls=%fused_computation.7 | loop fusion | flops 16 | bytes 256 | tf_op jit(solution)/shard_map/slice | solution.py:371
  4.5 0.1 concatenate.30
  4.6 0.8 %fusion = (f32[16]{0:T(128)S(1)}, f32[16]{0:T(128)S(1)}) fusion(f32[96]{0:T(128)} %param.31), kind=kLoop, calls=%fused_computation.6 | loop fusion | flops 16 | bytes 256 | tf_op jit(solution)/shard_map/slice | solution.py:371
  5.4 0.1 concatenate.33
  5.5 1.1 %copy.23.qup = bf16[512,192]{1,0:T(8,128)(2,1)S(1)} copy(bf16[512,192]{0,1:T(8,128)(2,1)} %param.27) | data formatting | bytes 393216 | tf_op args[7]
  6.6 1.2 %copy.22.rdown = bf16[2048,32]{1,0:T(8,128)(2,1)S(1)} copy(bf16[2048,32]{0,1:T(8,128)(2,1)} %param.24) | data formatting | bytes 262144 | tf_op args[4]
  7.8 0.0 copy-start
  7.8 1.6 %copy-done = bf16[2048,512]{1,0:T(8,128)(2,1)S(1)} copy-done((bf16[2048,512]{1,0:T(8,128)(2,1)S(1)}, bf16[2048,512]{1,0:T(8,128)(2,1)}, u32[]{:S(2)}) %copy-start) | copy-done | bytes 2097176
  9.3 0.0 copy-start.1
  9.4 1.2 %copy-done.1 = bf16[2048,256]{1,0:T(8,128)(2,1)S(1)} copy-done((bf16[2048,256]{1,0:T(8,128)(2,1)S(1)}, bf16[2048,256]{1,0:T(8,128)(2,1)}, u32[]{:S(2)}) %copy-start.1) | copy-done | bytes 1048600
  10.6 0.0 copy-start.2
  10.6 1.0 %copy-done.2 = bf16[512,512]{1,0:T(8,128)(2,1)S(1)} copy-done((bf16[512,512]{1,0:T(8,128)(2,1)S(1)}, bf16[512,512]{1,0:T(8,128)(2,1)}, u32[]{:S(2)}) %copy-start.2) | copy-done | bytes 524312
  11.6 0.0 copy-start.3
  11.6 0.9 %copy-done.3 = bf16[128,1024]{1,0:T(8,128)(2,1)S(1)} copy-done((bf16[128,1024]{1,0:T(8,128)(2,1)S(1)}, bf16[128,1024]{1,0:T(8,128)(2,1)}, u32[]{:S(2)}) %copy-start.3) | copy-done | bytes 262168
  12.6 0.0 copy-start.4
  12.6 0.9 %copy-done.4 = bf16[192,384]{1,0:T(8,128)(2,1)S(1)} copy-done((bf16[192,384]{1,0:T(8,128)(2,1)S(1)}, bf16[192,384]{1,0:T(8,128)(2,1)}, u32[]{:S(2)}) %copy-start.4) | copy-done | bytes 147480
  13.5 0.0 copy-start.5
  13.5 0.9 %copy-done.5 = bf16[32,2048]{1,0:T(8,128)(2,1)S(1)} copy-done((bf16[32,2048]{1,0:T(8,128)(2,1)S(1)}, bf16[32,2048]{1,0:T(8,128)(2,1)}, u32[]{:S(2)}) %copy-start.5) | copy-done | bytes 131096
  14.4 0.0 copy-start.6
  14.4 0.9 %copy-done.6 = bf16[256,256]{1,0:T(8,128)(2,1)S(1)} copy-done((bf16[256,256]{1,0:T(8,128)(2,1)S(1)}, bf16[256,256]{1,0:T(8,128)(2,1)}, u32[]{:S(2)}) %copy-start.6) | copy-done | bytes 131096
  15.3 0.0 copy-start.7
  15.3 0.9 %copy-done.7 = bf16[256,256]{1,0:T(8,128)(2,1)S(1)} copy-done((bf16[256,256]{1,0:T(8,128)(2,1)S(1)}, bf16[256,256]{1,0:T(8,128)(2,1)}, u32[]{:S(2)}) %copy-start.7) | copy-done | bytes 131096
  16.2 0.0 copy-start.8
  16.2 0.9 %copy-done.8 = f32[2,128,128]{2,1,0:T(8,128)S(1)} copy-done((f32[2,128,128]{2,1,0:T(8,128)S(1)}, f32[2,128,128]{2,1,0:T(8,128)}, u32[]{:S(2)}) %copy-start.8) | copy-done | bytes 131096
  17.1 0.0 copy-start.9
  17.1 0.9 %copy-done.9 = f32[2,128,128]{2,1,0:T(8,128)S(1)} copy-done((f32[2,128,128]{2,1,0:T(8,128)S(1)}, f32[2,128,128]{2,1,0:T(8,128)}, u32[]{:S(2)}) %copy-start.9) | copy-done | bytes 131096
  18.0 0.0 copy-start.10
  18.0 0.8 %copy-done.10 = bf16[256,128]{1,0:T(8,128)(2,1)S(1)} copy-done((bf16[256,128]{1,0:T(8,128)(2,1)S(1)}, bf16[256,128]{1,0:T(8,128)(2,1)}, u32[]{:S(2)}) %copy-start.10) | copy-done | bytes 65560
  18.8 0.0 copy-start.11
  18.8 0.8 %copy-done.11 = bf16[256,128]{1,0:T(8,128)(2,1)S(1)} copy-done((bf16[256,128]{1,0:T(8,128)(2,1)S(1)}, bf16[256,128]{1,0:T(8,128)(2,1)}, u32[]{:S(2)}) %copy-start.11) | copy-done | bytes 65560
  19.7 0.0 copy-start.12
  19.7 0.7 copy-done.12
  20.4 0.0 copy-start.13
  20.4 0.7 copy-done.13
  21.0 0.0 copy-start.14
  21.0 0.7 copy-done.14
  21.7 0.0 copy-start.15
  21.7 0.7 copy-done.15
  22.4 53.3 %shard_map.203 = (bf16[128,512]{1,0:T(8,128)(2,1)S(1)}, f32[2,128]{1,0:T(2,128)S(1)}) custom-call(bf16[32,2048]{1,0:T(8,128)(2,1)S(1)} %copy-done.5, s32[16]{0:T(128)S(1)} %copy-done.15, bf16[2048,512]{1,0:T(8,128)(2,1)S(1)} %copy-done, bf16[2048,256]{1,0:T(8,128)(2,1)S(1)} %copy-done.1, bf16[2048,32]{1,0:T(8,128)(2,1)S(1)} %copy.22.rdown, ...), custom_call_target="tpu_custom_call" | custom-call | tf_op jit(solution)/shard_map/pallas_call | solution.py:394
  75.7 0.7 copy.26
  76.4 0.6 copy.27
  (2 shorter events, 0.0 us)
Async XLA Ops:
  7.8 1.6 %copy-start = (bf16[2048,512]{1,0:T(8,128)(2,1)S(1)}, bf16[2048,512]{1,0:T(8,128)(2,1)}, u32[]{:S(2)}) copy-start(bf16[2048,512]{1,0:T(8,128)(2,1)} %qdown.1) | copy-start | bytes 6291460
  9.3 1.2 %copy-start.1 = (bf16[2048,256]{1,0:T(8,128)(2,1)S(1)}, bf16[2048,256]{1,0:T(8,128)(2,1)}, u32[]{:S(2)}) copy-start(bf16[2048,256]{1,0:T(8,128)(2,1)} %ldown.1) | copy-start | bytes 3145732
  10.6 1.0 %copy-start.2 = (bf16[512,512]{1,0:T(8,128)(2,1)S(1)}, bf16[512,512]{1,0:T(8,128)(2,1)}, u32[]{:S(2)}) copy-start(bf16[512,512]{1,0:T(8,128)(2,1)} %oweight.1) | copy-start | bytes 1572868
  11.6 0.9 %copy-start.3 = (bf16[128,1024]{1,0:T(8,128)(2,1)S(1)}, bf16[128,1024]{1,0:T(8,128)(2,1)}, u32[]{:S(2)}) copy-start(bf16[128,1024]{1,0:T(8,128)(2,1)} %constant.17.clone.spread) | copy-start | bytes 786436
  12.6 0.9 %copy-start.4 = (bf16[192,384]{1,0:T(8,128)(2,1)S(1)}, bf16[192,384]{1,0:T(8,128)(2,1)}, u32[]{:S(2)}) copy-start(bf16[192,384]{1,0:T(8,128)(2,1)} %constant.16.clone.qcols) | copy-start | bytes 442372
  13.5 0.9 %copy-start.5 = (bf16[32,2048]{1,0:T(8,128)(2,1)S(1)}, bf16[32,2048]{1,0:T(8,128)(2,1)}, u32[]{:S(2)}) copy-start(bf16[32,2048]{1,0:T(8,128)(2,1)} %tok.1) | copy-start | bytes 393220
  14.4 0.9 %copy-start.6 = (bf16[256,256]{1,0:T(8,128)(2,1)S(1)}, bf16[256,256]{1,0:T(8,128)(2,1)}, u32[]{:S(2)}) copy-start(bf16[256,256]{1,0:T(8,128)(2,1)} %constant.19.clone.qsum) | copy-start | bytes 393220
  15.3 0.9 %copy-start.7 = (bf16[256,256]{1,0:T(8,128)(2,1)S(1)}, bf16[256,256]{1,0:T(8,128)(2,1)}, u32[]{:S(2)}) copy-start(bf16[256,256]{1,0:T(8,128)(2,1)} %constant.18.clone.ksum) | copy-start | bytes 393220
  16.2 0.9 %copy-start.8 = (f32[2,128,128]{2,1,0:T(8,128)S(1)}, f32[2,128,128]{2,1,0:T(8,128)}, u32[]{:S(2)}) copy-start(f32[2,128,128]{2,1,0:T(8,128)} %constant.15.clone.coarse) | copy-start | bytes 393220
  17.1 0.9 %copy-start.9 = (f32[2,128,128]{2,1,0:T(8,128)S(1)}, f32[2,128,128]{2,1,0:T(8,128)}, u32[]{:S(2)}) copy-start(f32[2,128,128]{2,1,0:T(8,128)} %constant.14.clone.fine) | copy-start | bytes 393220
  18.0 0.8 %copy-start.10 = (bf16[256,128]{1,0:T(8,128)(2,1)S(1)}, bf16[256,128]{1,0:T(8,128)(2,1)}, u32[]{:S(2)}) copy-start(bf16[256,128]{1,0:T(8,128)(2,1)} %kup.1) | copy-start | bytes 196612
  18.8 0.8 %copy-start.11 = (bf16[256,128]{1,0:T(8,128)(2,1)S(1)}, bf16[256,128]{1,0:T(8,128)(2,1)}, u32[]{:S(2)}) copy-start(bf16[256,128]{1,0:T(8,128)(2,1)} %vup.1) | copy-start | bytes 196612
  19.7 0.7 copy-start.12
  20.4 0.7 copy-start.13
  21.0 0.7 copy-start.14
  21.7 0.7 copy-start.15

commit v2 on v1

v2 whole, which is shorter than its diff:
```python
import functools

import jax
import jax.numpy as jnp
import numpy as np
from jax import lax
from jax.experimental import pallas as pl
from jax.experimental.pallas import tpu as pltpu
from jax.sharding import PartitionSpec as P

NOPE = 64
ROPE = 32
VD = 64
NDOC = 16
WIDTH = NOPE + ROPE
EPS = 1e-06
THETA = 10000.0
APART = -float(2**20)
SCALE = WIDTH**-0.5
LOG2E = 1.4426950408889634
F32 = jnp.float32
BF16 = jnp.bfloat16
MESH = pl.DeviceIdType.MESH
DOC_LANE = 64


def split_of(count):
    return {128: (8, 8, 2), 8: (2, 2, 2), 16: (2, 4, 2)}[count]


def tables(blocks):
    half = ROPE // 2
    inverse = THETA ** (-(np.arange(128) % half).astype(np.float64) / half)
    fine = np.arange(128)[:, None] * inverse[None]
    coarse = (np.arange(blocks) * 128)[:, None] * inverse[None]
    fine = np.stack([np.cos(fine), np.sin(fine)]).astype(np.float32)
    coarse = np.stack([np.cos(coarse), np.sin(coarse)]).astype(np.float32)
    return fine, coarse


def query_columns():
    out = np.zeros((2 * WIDTH, 384), np.float32)
    for j in range(128):
        out[(j // 64) * WIDTH + j % 64, j] = 1
        head, entry = (j % 64) // 32, j % 32
        out[head * WIDTH + NOPE + entry, 128 + j] = 1
        out[head * WIDTH + NOPE + (entry + 16) % 32, 256 + j] = 1
    return out


def rope_spread():
    out = np.zeros((128, 1024), np.float32)
    for g in range(4):
        for j in range(64):
            out[32 * g + j % 32, 256 * g + j] = 1
            out[32 * g + (j % 32 + 16) % 32, 256 * g + 128 + j] = 1
    return out


def sum_matrix(rope_lanes):
    out = np.zeros((256, 256), np.float32)
    for col in range(256):
        head = col // 64 if col < 128 else ((col - 128) // 32) % 2
        for i in range(128):
            out[i, col] = i // 64 == head
        for i in range(64):
            if rope_lanes == 32:
                out[128 + i, col] = i < 32
            else:
                out[128 + i, col] = i // 32 == head
    return out


def dot(a, b):
    return jnp.dot(a, b, preferred_element_type=F32)


def dot_t(a, b):
    return lax.dot_general(a, b, (((1,), (1,)), ((), ())), preferred_element_type=F32)


def lanes(rows, width=128):
    return lax.broadcasted_iota(jnp.int32, (rows, width), 1)


def rows_of(rows, width=128):
    return lax.broadcasted_iota(jnp.int32, (rows, width), 0)


def head_sums(squares, matrix):
    high = squares.astype(BF16)
    low = (squares - high.astype(F32)).astype(BF16)
    return dot(high, matrix) + dot(low, matrix)


def offsets(count):
    return [(i + 1) // 2 if i % 2 else (count - i // 2) % count for i in range(count)]


def gain_columns():
    out = np.zeros((WIDTH, 384), np.float32)
    for j in range(128):
        entry = j % 32
        out[j % 64, j] = 1
        out[NOPE + entry, 128 + j] = 1
        out[NOPE + (entry + 16) % 32, 256 + j] = -1 if entry < 16 else 1
    return out


def kernel(
    Z, Y, C, X, batches,
    tok_h, doclen, qdown_h, ldown_h, rdown_h, qlgain_h, lgain_h, qup_h, kup_h, vup_h, qgain_h, kgain_h, ogain_h, oweight_h,
    fine_h, coarse_h, qcols_h, spread_h, ksum_h, qsum_h, gcols_h,
    out, logs,
    tok, qdown, ldown, rdown, qlgain, lgain, qup, kup, vup, qgain, kgain, ogain, oweight,
    fine, coarse, qcols, spread, ksum, qsum, gcols,
    qlbuf, klbuf, rkbuf, qbuf, kall, vtall, sbuf, vupt, osend, lsend, orecv, lrecv, hobuf, bounds, gains,
    in_s, ql_s, ql_r, kz_s, kz_r, kx_s, kx_r, kf_s, kf_r, kc_s, kc_r, qy_s, qy_r, o_s, o_r, ho_s, ho_r,
):
    s = lax.axis_index("sp")
    t = lax.axis_index("tp")
    z = s // (Y * C)
    y = lax.rem(s // C, Y)
    c = lax.rem(s, C)
    gz = Z * 32
    groups = C * X

    def at(zz, yy, cc):
        return (zz * Y + yy) * C + cc

    def zpeer(k):
        return at(lax.rem(z + k, Z), y, c), t

    def ypeer(k):
        yy = lax.rem(y + k, Y)
        return yy, (at(z, yy, c), t)

    def xof(k):
        return lax.rem(t + k + X, X)

    def xpeer(k):
        return s, xof(k)

    other = (at(z, y, 1 - c), t)

    def remote(src, dst, ss, rs, who):
        return pltpu.make_async_remote_copy(
            src_ref=src, dst_ref=dst, send_sem=ss, recv_sem=rs, device_id=who, device_id_type=MESH
        )

    barrier = pltpu.get_barrier_semaphore()
    peers = [zpeer(k) for k in range(1, Z)] + [ypeer(k)[1] for k in range(1, Y)]
    peers += [xpeer(k) for k in range(1, X)] + [other]
    for who in peers:
        pl.semaphore_signal(barrier, inc=1, device_id=who, device_id_type=MESH)

    pairs = [
        (tok_h, tok), (qdown_h, qdown), (qlgain_h, qlgain), (ldown_h, ldown), (lgain_h, lgain), (rdown_h, rdown),
        (qup_h, qup), (qcols_h, qcols), (qgain_h, qgain), (kgain_h, kgain), (gcols_h, gcols), (vup_h, vup),
        (fine_h, fine), (coarse_h, coarse), (qsum_h, qsum), (kup_h, kup), (spread_h, spread), (ksum_h, ksum),
        (ogain_h, ogain), (oweight_h, oweight),
    ]
    loads = [pltpu.make_async_copy(a, b, in_s.at[i]) for i, (a, b) in enumerate(pairs)]
    for load in loads:
        load.start()
    sends = []

    def post(copy):
        copy.start()
        sends.append(copy)

    for load in loads[0:3]:
        load.wait()
    x = tok[...]
    qd = dot(x, qdown[...])
    qd = qd * lax.rsqrt(jnp.mean(qd * qd, axis=-1, keepdims=True) + EPS) * qlgain[...]
    qlbuf[t] = qd.astype(BF16)
    for load in loads[3:6]:
        load.wait()
    kd = dot(x, ldown[...])
    kd = kd * lax.rsqrt(jnp.mean(kd * kd, axis=-1, keepdims=True) + EPS) * lgain[...]
    klbuf[t, 0] = kd.astype(BF16)
    rope = rdown[...]
    rk4 = dot_t(x, jnp.concatenate([rope, rope, rope, rope], axis=0)).astype(BF16).astype(F32)
    group = lanes(8) // 32
    rkbuf[t, 0] = jnp.where(
        group == 0, rk4[0:8], jnp.where(group == 1, rk4[8:16], jnp.where(group == 2, rk4[16:24], rk4[24:32]))
    )

    pl.semaphore_wait(barrier, len(peers))

    for k in range(1, X):
        post(remote(qlbuf.at[t], qlbuf.at[t], ql_s.at[k], ql_r.at[k], xpeer(k)))
    order = offsets(Z)
    for i in range(1, Z):
        back = order.index((Z - order[i]) % Z)
        for n, buf in enumerate((klbuf, rkbuf)):
            post(remote(buf.at[t, 0], buf.at[t, back], kz_s.at[n, i], kz_r.at[n, back], zpeer(order[i])))

    def to_x(i):
        first, count = batches[i]
        for n, buf in enumerate((klbuf, rkbuf)):
            part = buf.at[t, pl.ds(first, count)]
            for d in range(2):
                post(remote(part, part, kx_s.at[n, d, i], kx_r.at[n, d, i], xpeer(1 - 2 * d)))

    to_x(0)

    for load in loads[6:]:
        load.wait()
    lane1 = lanes(1)
    starts = jnp.full((1, 128), 1 << 30, jnp.int32)
    ends = jnp.zeros((1, 128), jnp.int32)
    total = jnp.int32(0)
    for d in range(NDOC):
        starts = jnp.where(lane1 == DOC_LANE + d, total, starts)
        total = total + doclen[d]
        ends = jnp.where(lane1 == DOC_LANE + d, total, ends)
    bounds[0:1, :] = starts
    bounds[1:2, :] = ends
    for n, gain in enumerate((qgain, kgain)):
        high = gain[...].astype(BF16)
        rest = gain[...] - high.astype(F32)
        middle = rest.astype(BF16)
        low = (rest - middle.astype(F32)).astype(BF16)
        spots = sum(dot(jnp.broadcast_to(piece, (8, WIDTH)), gcols[...]) for piece in (high, middle, low))
        for i in range(3):
            gains[3 * n + i : 3 * n + i + 1, :] = spots[0:1, 128 * i : 128 * i + 128]
    qweight = dot(qcols[...], qup[...]).astype(BF16)
    vupt[...] = jnp.transpose(vup[...].astype(F32)).astype(BF16)

    def turn(block, first, count):
        cb = coarse[0, pl.ds(block, 1), :]
        sb = coarse[1, pl.ds(block, 1), :]
        cf = fine[0, pl.ds(first, count), :]
        sf = fine[1, pl.ds(first, count), :]
        return cb * cf - sb * sf, sb * cf + cb * sf

    for k in range(1, X):
        xx = xof(-k)
        remote(qlbuf.at[xx], qlbuf.at[xx], ql_s.at[k], ql_r.at[k], (s, xx)).wait_recv()
    ql = qlbuf[...].reshape(128, qlbuf.shape[2])
    qq = dot_t(ql, qweight)
    q0, q1, q2 = qq[:, 0:128], qq[:, 128:256], qq[:, 256:384]
    qs = head_sums(jnp.concatenate([q0 * q0, q1 * q1], axis=1), qsum[...])
    qs = lax.rsqrt(qs * (1.0 / WIDTH) + EPS)
    cosine, sine = turn(s, 0, 128)
    plain = q0 * qs[:, 0:128] * gains[0:1, :]
    rope = (q1 * gains[1:2, :] * cosine + q2 * gains[2:3, :] * sine) * qs[:, 128:256]
    qbuf[y, 0:128, :] = plain.astype(BF16)
    qbuf[y, 128:192, :] = jnp.where(lanes(64) < 64, rope[0:64], rope[64:128]).astype(BF16)
    for k in offsets(Y)[1:]:
        post(remote(qbuf.at[y], qbuf.at[y], qy_s.at[k], qy_r.at[k], ypeer(k)[1]))

    for i in range(1, len(batches)):
        first, count = batches[i]
        for slot in range(first, first + count):
            for n, buf in enumerate((klbuf, rkbuf)):
                remote(buf.at[t, 0], buf.at[t, slot], kz_s.at[n, slot], kz_r.at[n, slot], zpeer(order[slot])).wait_recv()
        to_x(i)

    def expand(xx):
        kl = klbuf[xx].reshape(gz, klbuf.shape[3])
        index = c * X + xx
        vtall[index] = dot_t(vupt[...], kl).astype(BF16)
        raw = dot(kl, kup[...])
        spreaded = dot(rkbuf[xx].reshape(Z * 8, 128).astype(BF16), spread[...])

        def rows_from(shift):
            return jnp.concatenate(
                [spreaded[8 * i : 8 * i + 8, 256 * g + shift : 256 * g + shift + 128] for i in range(Z) for g in range(4)],
                axis=0,
            )

        r1, r2 = rows_from(0), rows_from(128)
        sums = head_sums(jnp.concatenate([raw * raw, r1 * r1], axis=1), ksum[...])
        sums = lax.rsqrt(sums * (1.0 / WIDTH) + EPS)
        kall[index, :, 0:128] = (raw * sums[:, 0:128] * gains[3:4, :]).astype(BF16)
        first = pl.multiple_of(xx * 32, 32)
        for i in range(Z):
            block = at(lax.rem(z + order[i], Z), y, c)
            cosine, sine = turn(block, first, 32)
            part = slice(i * 32, i * 32 + 32)
            turned = (r1[part] * gains[4:5, :] * cosine + r2[part] * gains[5:6, :] * sine) * sums[part, 128:256]
            place = block * 128 + first + rows_of(32)
            inside = (place >= bounds[0:1, :]) & (place < bounds[1:2, :])
            kall[index, part, 128:256] = jnp.where(inside, 1.0, turned).astype(BF16)

    def to_core(xx):
        index = c * X + xx
        for n, buf in enumerate((kall, vtall)):
            post(remote(buf.at[index], buf.at[index], kc_s.at[n, xx], kc_r.at[n, xx], other))

    expand(t)
    for i, (first, count) in enumerate(batches):
        for d in range(2):
            xx = xof(2 * d - 1)
            for n, buf in enumerate((klbuf, rkbuf)):
                part = buf.at[xx, pl.ds(first, count)]
                remote(part, part, kx_s.at[n, d, i], kx_r.at[n, d, i], (s, xx)).wait_recv()
                if d == onward(i):
                    post(remote(part, part, kf_s.at[n, i], kf_r.at[n, i], xpeer(1 - 2 * d)))
    to_core(t)
    expand(xof(-1))
    expand(xof(1))
    for i, (first, count) in enumerate(batches):
        xx = xof(2)
        for n, buf in enumerate((klbuf, rkbuf)):
            part = buf.at[xx, pl.ds(first, count)]
            remote(part, part, kf_s.at[n, i], kf_r.at[n, i], xpeer(2 * onward(i) - 1)).wait_recv()
    to_core(xof(-1))
    to_core(xof(1))
    expand(xof(2))
    to_core(xof(2))
    for xx in range(X):
        index = (1 - c) * X + xx
        for n, buf in enumerate((kall, vtall)):
            remote(buf.at[index], buf.at[index], kc_s.at[n, xx], kc_r.at[n, xx], other).wait_recv()

    def attend(yy):
        block = at(z, yy, c)
        qplain = qbuf[yy, 0:128, :].astype(F32)
        qrope = qbuf[yy, 128:192, :].astype(F32)
        qrope = jnp.concatenate([qrope, pltpu.roll(qrope, 64, 1)], axis=0)
        place = block * 128 + rows_of(128)
        inside = (place >= bounds[0:1, :]) & (place < bounds[1:2, :])
        lane = lanes(128)
        apart = jnp.where((lane >= DOC_LANE) & (lane < DOC_LANE + NDOC) & jnp.logical_not(inside), APART, 0.0)
        both = []
        for h in range(2):
            left = jnp.where(lane // 64 == h, qplain, 0.0)
            right = jnp.where(lane // 32 == h, qrope, apart)
            both.append(jnp.concatenate([left, right], axis=1))
        queries = jnp.concatenate(both, axis=0).astype(BF16)
        scores = dot_t(kall[...].reshape(groups * gz, 256), queries)
        sbuf[...] = scores.reshape(groups, gz, 256)
        top = jnp.max(scores, axis=0, keepdims=True)
        count = None
        acc = None
        for g in range(groups):
            weights = jnp.exp2((sbuf[g] - top) * (SCALE * LOG2E))
            added = jnp.sum(weights, axis=0, keepdims=True)
            count = added if count is None else count + added
            update = dot(vtall[g], weights.astype(BF16))
            acc = update if acc is None else acc + update
        log = top * SCALE + jnp.log(count)
        lsend[yy] = jnp.where(rows_of(8) == 0, log[:, 0:128], log[:, 128:256])
        inv = 1.0 / count
        osend[yy, 0:64, :] = (acc[0:64, 0:128] * inv[:, 0:128]).astype(BF16)
        osend[yy, 64:128, :] = (acc[64:128, 128:256] * inv[:, 128:256]).astype(BF16)

    def step(i, carry):
        k = lax.rem(jnp.where(lax.rem(i, 2) == 1, (i + 1) // 2, Y - i // 2), Y)
        yy, who = ypeer(k)
        back = lax.rem(Y - k, Y)

        @pl.when(i > 0)
        def _():
            remote(qbuf.at[yy], qbuf.at[yy], qy_s.at[back], qy_r.at[back], who).wait_recv()

        attend(yy)

        @pl.when(i > 0)
        def _():
            remote(osend.at[yy], orecv.at[y], o_s.at[0, k], o_r.at[0, k], who).start()
            remote(lsend.at[yy], lrecv.at[y], o_s.at[1, k], o_r.at[1, k], who).start()

        return carry

    lax.fori_loop(0, Y, step, 0)

    orecv[y] = osend[y]
    lrecv[y] = lsend[y]
    for k in range(1, Y):
        yy, who = ypeer(Y - k)
        remote(osend.at[yy], orecv.at[yy], o_s.at[0, k], o_r.at[0, k], who).wait_recv()
        remote(lsend.at[yy], lrecv.at[yy], o_s.at[1, k], o_r.at[1, k], who).wait_recv()
    top = lrecv[0]
    for i in range(1, Y):
        top = jnp.maximum(top, lrecv[i])
    whole = jnp.zeros_like(top)
    acc0 = jnp.zeros((64, 128), F32)
    acc1 = jnp.zeros((64, 128), F32)
    for i in range(Y):
        weight = jnp.exp(lrecv[i] - top)
        whole = whole + weight
        acc0 = acc0 + weight[0:1] * orecv[i, 0:64, :].astype(F32)
        acc1 = acc1 + weight[1:2] * orecv[i, 64:128, :].astype(F32)
    logs[...] = (top + jnp.log(whole))[0:2]
    inv = 1.0 / whole
    heads = jnp.concatenate([acc0 * inv[0:1], acc1 * inv[1:2]], axis=0)
    hobuf[t] = jnp.transpose(heads).astype(BF16)
    for k in range(1, X):
        post(remote(hobuf.at[t], hobuf.at[t], ho_s.at[k], ho_r.at[k], xpeer(k)))
    for k in range(1, Y):
        yy, who = ypeer(k)
        remote(osend.at[yy], orecv.at[y], o_s.at[0, k], o_r.at[0, k], who).wait_send()
        remote(lsend.at[yy], lrecv.at[y], o_s.at[1, k], o_r.at[1, k], who).wait_send()
    for k in range(1, X):
        xx = xof(-k)
        remote(hobuf.at[xx], hobuf.at[xx], ho_s.at[k], ho_r.at[k], (s, xx)).wait_recv()
    full = jnp.concatenate([hobuf[i].astype(F32) for i in range(X)], axis=1)
    normed = full * lax.rsqrt(jnp.mean(full * full, axis=-1, keepdims=True) + EPS) * ogain[...]
    out[...] = dot(normed.astype(BF16), oweight[...]).astype(BF16)
    for copy in sends:
        copy.wait_send()


def onward(batch):
    return 0 if batch in (0, 3) else 1


def per_device(
    split, X,
    tokens, doc_lengths, query_down, latent_down, rope_down, query_latent_gain, latent_gain,
    query_up, key_up, value_up, query_gain, key_gain, output_gain, output_weight,
):
    Z, Y, C = split
    fine, coarse = tables(Z * Y * C)
    hbm = pl.BlockSpec(memory_space=pltpu.HBM)
    vm = pl.BlockSpec(memory_space=pltpu.VMEM)
    sm = pl.BlockSpec(memory_space=pltpu.SMEM)
    dma = pltpu.SemaphoreType.DMA
    gz = Z * 32
    groups = C * X
    batches = [(0, 1), (1, 2), (3, 2), (5, 3)] if Z == 8 else [(0, 1), (1, 1)]
    QR, KVR = query_down.shape[1], latent_down.shape[1]
    const = lambda a: jnp.asarray(a, BF16)
    row = lambda a: a.reshape(1, -1)
    inputs = [
        tokens, query_down, latent_down, rope_down.T, row(query_latent_gain), row(latent_gain),
        query_up.T, key_up, value_up, row(query_gain), row(key_gain), row(output_gain), output_weight,
        jnp.asarray(fine), jnp.asarray(coarse), const(query_columns().T), const(rope_spread()),
        const(sum_matrix(32)), const(sum_matrix(64)), const(gain_columns()),
    ]
    return pl.pallas_call(
        functools.partial(kernel, Z, Y, C, X, batches),
        out_shape=(
            jax.ShapeDtypeStruct((128, output_weight.shape[1]), BF16),
            jax.ShapeDtypeStruct((2, 128), F32),
        ),
        in_specs=[hbm, sm] + [hbm] * (len(inputs) - 1),
        out_specs=(vm, vm),
        scratch_shapes=[pltpu.VMEM(a.shape, a.dtype) for a in inputs] + [
            pltpu.VMEM((X, 32, QR), BF16),
            pltpu.VMEM((X, Z, 32, KVR), BF16),
            pltpu.VMEM((X, Z, 8, 128), F32),
            pltpu.VMEM((Y, 192, 128), BF16),
            pltpu.VMEM((groups, gz, 256), BF16),
            pltpu.VMEM((groups, 128, gz), BF16),
            pltpu.VMEM((groups, gz, 256), F32),
            pltpu.VMEM((128, KVR), BF16),
            pltpu.VMEM((Y, 128, 128), BF16),
            pltpu.VMEM((Y, 8, 128), F32),
            pltpu.VMEM((Y, 128, 128), BF16),
            pltpu.VMEM((Y, 8, 128), F32),
            pltpu.VMEM((X, 128, 128), BF16),
            pltpu.VMEM((8, 128), jnp.int32),
            pltpu.VMEM((8, 128), F32),
            dma((len(inputs),)),
            dma((X,)), dma((X,)),
            dma((2, Z)), dma((2, Z)),
            dma((2, 2, 4)), dma((2, 2, 4)),
            dma((2, 4)), dma((2, 4)),
            dma((2, X)), dma((2, X)),
            dma((Y,)), dma((Y,)),
            dma((2, Y)), dma((2, Y)),
            dma((X,)), dma((X,)),
        ],
        compiler_params=pltpu.CompilerParams(
            collective_id=0, has_side_effects=True, vmem_limit_bytes=60 * 2**20
        ),
    )(tokens, doc_lengths, *inputs[1:])


def solution(mesh):
    split = split_of(mesh.shape["sp"])
    return jax.shard_map(
        functools.partial(per_device, split, mesh.shape["tp"]),
        mesh=mesh,
        in_specs=(
            P(("sp", "tp"), None),
            P(), P(), P(), P(), P(), P(),
            P(None, "tp"), P(None, "tp"), P(None, "tp"),
            P(), P(), P(),
            P(None, "tp"),
        ),
        out_specs=(P("sp", "tp"), P("tp", "sp")),
        check_vma=False,
    )
```

time: 77.6 us -> 56.7 us (0.73)
  the two profiles are of different devices: /device:TPU:8 before, /device:TPU:1 now
where the time goes in v2:
time: 56.7 us; the launch traced here: 56.6 us
  Pallas kernels  53.1 us (94%)
  local copies, waits for them, and re-layouts  2.8 us (5%)
  between operations  0.64 us (1%)
    pallas_call x1, Pallas kernels, per_device(): pl.pallas_call(functools.partial(kernel, Z, Y, C, X, batches), out_shape=...  53.1 us
    unnamed x2, local copies, waits for them, and re-layouts  2.8 us

profile of v2, /device:TPU:1, one launch (start us, length us, event | category | flops | bytes accessed | tf_op | source)
XLA Modules:
  0.0 56.6 jit_solution(7250540110547514528)
XLA Ops:
  0.6 53.1 %shard_map.212 = (bf16[128,512]{1,0:T(8,128)(2,1)}, f32[2,128]{1,0:T(2,128)}) custom-call(bf16[32,2048]{1,0:T(8,128)(2,1)} %tok_h.1, s32[16]{0:T(128)} %doclen.1, bf16[2048,512]{1,0:T(8,128)(2,1)} %qdown_h.1, bf16[2048,256]{1,0:T(8,128)(2,1)} %ldown_h.1, bf16[32,2048]{1,0:T(8,128)(2,1)} %bitcast.8, f32[1,512]{1,0:T(1,128)} %bitcast.9, f32[1,256]{1,0:T(1,128)} %bitcast.11, ...), custom_call_target="tpu_custom_call" | custom-call | tf_op jit(solution)/shard_map/pallas_call | solution.py:436
  53.8 1.6 %copy.25 = bf16[128,512]{1,0:T(8,128)(2,1)} copy(bf16[128,512]{1,0:T(8,128)(2,1)} %get-tuple-element.4) | data formatting | bytes 262144
  55.4 1.2 %copy.26 = f32[2,128]{1,0:T(2,128)} copy(f32[2,128]{1,0:T(2,128)} %get-tuple-element.5) | data formatting | bytes 2048

commit v3 on v2

--- a/solution.py
+++ b/solution.py
@@ -38,13 +38,14 @@
     return fine, coarse
 
 
-def query_columns():
-    out = np.zeros((2 * WIDTH, 384), np.float32)
+def query_rows():
+    out = np.zeros((256, 2 * WIDTH), np.float32)
     for j in range(128):
-        out[(j // 64) * WIDTH + j % 64, j] = 1
-        head, entry = (j % 64) // 32, j % 32
-        out[head * WIDTH + NOPE + entry, 128 + j] = 1
-        out[head * WIDTH + NOPE + (entry + 16) % 32, 256 + j] = 1
+        out[j, (j // 64) * WIDTH + j % 64] = 1
+    for j in range(64):
+        head, entry = j // 32, j % 32
+        out[128 + j, head * WIDTH + NOPE + entry] = 1
+        out[192 + j, head * WIDTH + NOPE + (entry + 16) % 32] = 1
     return out
 
 
@@ -57,17 +58,13 @@
     return out
 
 
-def sum_matrix(rope_lanes):
+def sum_matrix():
     out = np.zeros((256, 256), np.float32)
     for col in range(256):
         head = col // 64 if col < 128 else ((col - 128) // 32) % 2
         for i in range(128):
             out[i, col] = i // 64 == head
-        for i in range(64):
-            if rope_lanes == 32:
-                out[128 + i, col] = i < 32
-            else:
-                out[128 + i, col] = i // 32 == head
+        out[128:160, col] = 1
     return out
 
 
@@ -110,11 +107,11 @@
 def kernel(
     Z, Y, C, X, batches,
     tok_h, doclen, qdown_h, ldown_h, rdown_h, qlgain_h, lgain_h, qup_h, kup_h, vup_h, qgain_h, kgain_h, ogain_h, oweight_h,
-    fine_h, coarse_h, qcols_h, spread_h, ksum_h, qsum_h, gcols_h,
+    fine_h, coarse_h, qcols_h, spread_h, ksum_h, gcols_h,
     out, logs,
     tok, qdown, ldown, rdown, qlgain, lgain, qup, kup, vup, qgain, kgain, ogain, oweight,
-    fine, coarse, qcols, spread, ksum, qsum, gcols,
-    qlbuf, klbuf, rkbuf, qbuf, kall, vtall, sbuf, vupt, osend, lsend, orecv, lrecv, hobuf, bounds, gains,
+    fine, coarse, qcols, spread, ksum, gcols,
+    qlbuf, klbuf, rkbuf, qbuf, kall, vtall, sbuf0, sbuf1, pbuf0, pbuf1, stats, qside, qtable, vupt, osend, lsend, orecv, lrecv, hobuf, bounds, columns, gains,
     in_s, ql_s, ql_r, kz_s, kz_r, kx_s, kx_r, kf_s, kf_r, kc_s, kc_r, qy_s, qy_r, o_s, o_r, ho_s, ho_r,
 ):
     s = lax.axis_index("sp")
@@ -148,35 +145,30 @@
             src_ref=src, dst_ref=dst, send_sem=ss, recv_sem=rs, device_id=who, device_id_type=MESH
         )
 
+    pairs = [
+        (tok_h, tok), (ldown_h, ldown), (lgain_h, lgain), (rdown_h, rdown), (qdown_h, qdown), (qlgain_h, qlgain),
+        (qup_h, qup), (qcols_h, qcols), (qgain_h, qgain), (kgain_h, kgain), (gcols_h, gcols), (vup_h, vup),
+        (fine_h, fine), (coarse_h, coarse), (kup_h, kup), (spread_h, spread), (ksum_h, ksum),
+        (ogain_h, ogain), (oweight_h, oweight),
+    ]
+    loads = [pltpu.make_async_copy(a, b, in_s.at[i]) for i, (a, b) in enumerate(pairs)]
+    for load in loads:
+        load.start()
     barrier = pltpu.get_barrier_semaphore()
     peers = [zpeer(k) for k in range(1, Z)] + [ypeer(k)[1] for k in range(1, Y)]
     peers += [xpeer(k) for k in range(1, X)] + [other]
     for who in peers:
         pl.semaphore_signal(barrier, inc=1, device_id=who, device_id_type=MESH)
 
-    pairs = [
-        (tok_h, tok), (qdown_h, qdown), (qlgain_h, qlgain), (ldown_h, ldown), (lgain_h, lgain), (rdown_h, rdown),
-        (qup_h, qup), (qcols_h, qcols), (qgain_h, qgain), (kgain_h, kgain), (gcols_h, gcols), (vup_h, vup),
-        (fine_h, fine), (coarse_h, coarse), (qsum_h, qsum), (kup_h, kup), (spread_h, spread), (ksum_h, ksum),
-        (ogain_h, ogain), (oweight_h, oweight),
-    ]
-    loads = [pltpu.make_async_copy(a, b, in_s.at[i]) for i, (a, b) in enumerate(pairs)]
-    for load in loads:
-        load.start()
     sends = []
 
     def post(copy):
         copy.start()
         sends.append(copy)
 
-    for load in loads[0:3]:
+    for load in loads[0:4]:
         load.wait()
     x = tok[...]
-    qd = dot(x, qdown[...])
-    qd = qd * lax.rsqrt(jnp.mean(qd * qd, axis=-1, keepdims=True) + EPS) * qlgain[...]
-    qlbuf[t] = qd.astype(BF16)
-    for load in loads[3:6]:
-        load.wait()
     kd = dot(x, ldown[...])
     kd = kd * lax.rsqrt(jnp.mean(kd * kd, axis=-1, keepdims=True) + EPS) * lgain[...]
     klbuf[t, 0] = kd.astype(BF16)
@@ -189,8 +181,6 @@
 
     pl.semaphore_wait(barrier, len(peers))
 
-    for k in range(1, X):
-        post(remote(qlbuf.at[t], qlbuf.at[t], ql_s.at[k], ql_r.at[k], xpeer(k)))
     order = offsets(Z)
     for i in range(1, Z):
         back = order.index((Z - order[i]) % Z)
@@ -205,6 +195,21 @@
                 post(remote(part, part, kx_s.at[n, d, i], kx_r.at[n, d, i], xpeer(1 - 2 * d)))
 
     to_x(0)
+
+    for load in loads[4:6]:
+        load.wait()
+    qd = dot(tok[...], qdown[...])
+    qd = qd * lax.rsqrt(jnp.mean(qd * qd, axis=-1, keepdims=True) + EPS) * qlgain[...]
+    qlbuf[t] = qd.astype(BF16)
+    for k in range(1, X):
+        post(remote(qlbuf.at[t], qlbuf.at[t], ql_s.at[k], ql_r.at[k], xpeer(k)))
+
+    def from_z(i):
+        first, count = batches[i]
+        for slot in range(first, first + count):
+            for n, buf in enumerate((klbuf, rkbuf)):
+                remote(buf.at[t, 0], buf.at[t, slot], kz_s.at[n, slot], kz_r.at[n, slot], zpeer(order[slot])).wait_recv()
+        to_x(i)
 
     for load in loads[6:]:
         load.wait()
@@ -218,6 +223,16 @@
         ends = jnp.where(lane1 == DOC_LANE + d, total, ends)
     bounds[0:1, :] = starts
     bounds[1:2, :] = ends
+    which = rows_of(NDOC)
+    total = jnp.int32(0)
+    starts = jnp.zeros((NDOC, 128), jnp.int32)
+    ends = jnp.zeros((NDOC, 128), jnp.int32)
+    for d in range(NDOC):
+        starts = jnp.where(which == d, total, starts)
+        total = total + doclen[d]
+        ends = jnp.where(which == d, total, ends)
+    columns[0] = starts
+    columns[1] = ends
     for n, gain in enumerate((qgain, kgain)):
         high = gain[...].astype(BF16)
         rest = gain[...] - high.astype(F32)
@@ -236,28 +251,31 @@
         sf = fine[1, pl.ds(first, count), :]
         return cb * cf - sb * sf, sb * cf + cb * sf
 
+    cosine, sine = turn(s, 0, 128)
+    qtable[0:64, :] = jnp.transpose(cosine * gains[1:2, :])[0:64, :]
+    qtable[64:128, :] = jnp.transpose(sine * gains[2:3, :])[0:64, :]
+    qtable[128:256, :] = jnp.transpose(jnp.broadcast_to(gains[0:1, :], (128, 128)))
+    qside[...] = jnp.zeros((256, 256), BF16)
+
+    from_z(1)
     for k in range(1, X):
         xx = xof(-k)
         remote(qlbuf.at[xx], qlbuf.at[xx], ql_s.at[k], ql_r.at[k], (s, xx)).wait_recv()
-    ql = qlbuf[...].reshape(128, qlbuf.shape[2])
-    qq = dot_t(ql, qweight)
-    q0, q1, q2 = qq[:, 0:128], qq[:, 128:256], qq[:, 256:384]
-    qs = head_sums(jnp.concatenate([q0 * q0, q1 * q1], axis=1), qsum[...])
-    qs = lax.rsqrt(qs * (1.0 / WIDTH) + EPS)
-    cosine, sine = turn(s, 0, 128)
-    plain = q0 * qs[:, 0:128] * gains[0:1, :]
-    rope = (q1 * gains[1:2, :] * cosine + q2 * gains[2:3, :] * sine) * qs[:, 128:256]
-    qbuf[y, 0:128, :] = plain.astype(BF16)
-    qbuf[y, 128:192, :] = jnp.where(lanes(64) < 64, rope[0:64], rope[64:128]).astype(BF16)
-    for k in offsets(Y)[1:]:
+    qq = dot_t(qweight, qlbuf[...].reshape(128, qlbuf.shape[2]))
+    for h in range(2):
+        q0 = qq[64 * h : 64 * h + 64]
+        q1 = qq[128 + 32 * h : 160 + 32 * h]
+        q2 = qq[192 + 32 * h : 224 + 32 * h]
+        qs = jnp.sum(q0 * q0, axis=0, keepdims=True) + jnp.sum(q1 * q1, axis=0, keepdims=True)
+        qs = lax.rsqrt(qs * (1.0 / WIDTH) + EPS)
+        qbuf[y, 64 * h : 64 * h + 64, :] = (q0 * qs * qtable[128 + 64 * h : 192 + 64 * h, :]).astype(BF16)
+        turned = q1 * qtable[32 * h : 32 * h + 32, :] + q2 * qtable[64 + 32 * h : 96 + 32 * h, :]
+        qbuf[y, 128 + 32 * h : 160 + 32 * h, :] = (turned * qs).astype(BF16)
+    for k in offsets(Y)[:0:-1]:
         post(remote(qbuf.at[y], qbuf.at[y], qy_s.at[k], qy_r.at[k], ypeer(k)[1]))
 
-    for i in range(1, len(batches)):
-        first, count = batches[i]
-        for slot in range(first, first + count):
-            for n, buf in enumerate((klbuf, rkbuf)):
-                remote(buf.at[t, 0], buf.at[t, slot], kz_s.at[n, slot], kz_r.at[n, slot], zpeer(order[slot])).wait_recv()
-        to_x(i)
+    for i in range(2, len(batches)):
+        from_z(i)
 
     def expand(xx):
         kl = klbuf[xx].reshape(gz, klbuf.shape[3])
@@ -317,57 +335,114 @@
         for n, buf in enumerate((kall, vtall)):
             remote(buf.at[index], buf.at[index], kc_s.at[n, xx], kc_r.at[n, xx], other).wait_recv()
 
-    def attend(yy):
-        block = at(z, yy, c)
-        qplain = qbuf[yy, 0:128, :].astype(F32)
-        qrope = qbuf[yy, 128:192, :].astype(F32)
-        qrope = jnp.concatenate([qrope, pltpu.roll(qrope, 64, 1)], axis=0)
-        place = block * 128 + rows_of(128)
-        inside = (place >= bounds[0:1, :]) & (place < bounds[1:2, :])
-        lane = lanes(128)
-        apart = jnp.where((lane >= DOC_LANE) & (lane < DOC_LANE + NDOC) & jnp.logical_not(inside), APART, 0.0)
-        both = []
+    sbufs, pbufs = (sbuf0, sbuf1), (pbuf0, pbuf1)
+
+    def turn_of(i):
+        j = Y - 1 - i
+        return lax.rem(jnp.where(lax.rem(j, 2) == 1, (j + 1) // 2, Y - j // 2), Y)
+
+    def prepare(i):
+        yy, _ = ypeer(turn_of(i))
+        place = at(z, yy, c) * 128 + lanes(NDOC)
+        inside = (place >= columns[0]) & (place < columns[1])
+        apart = jnp.where(inside, 0.0, APART).astype(BF16)
         for h in range(2):
-            left = jnp.where(lane // 64 == h, qplain, 0.0)
-            right = jnp.where(lane // 32 == h, qrope, apart)
-            both.append(jnp.concatenate([left, right], axis=1))
-        queries = jnp.concatenate(both, axis=0).astype(BF16)
-        scores = dot_t(kall[...].reshape(groups * gz, 256), queries)
-        sbuf[...] = scores.reshape(groups, gz, 256)
-        top = jnp.max(scores, axis=0, keepdims=True)
-        count = None
-        acc = None
-        for g in range(groups):
-            weights = jnp.exp2((sbuf[g] - top) * (SCALE * LOG2E))
-            added = jnp.sum(weights, axis=0, keepdims=True)
-            count = added if count is None else count + added
-            update = dot(vtall[g], weights.astype(BF16))
-            acc = update if acc is None else acc + update
-        log = top * SCALE + jnp.log(count)
+            cols = slice(128 * h, 128 * h + 128)
+            qside[64 * h : 64 * h + 64, cols] = qbuf[yy, 64 * h : 64 * h + 64, :]
+            qside[128 + 32 * h : 160 + 32 * h, cols] = qbuf[yy, 128 + 32 * h : 160 + 32 * h, :]
+            qside[128 + DOC_LANE : 128 + DOC_LANE + NDOC, cols] = apart
+    def score(par, g, most):
+        scores = dot(kall[g], qside[...])
+        for r in range(gz // 8):
+            part = scores[8 * r : 8 * r + 8]
+            sbufs[par][g, 8 * r : 8 * r + 8, :] = part
+            most[r % 2] = part if most[r % 2] is None else jnp.maximum(most[r % 2], part)
+
+    def scored(par, most):
+        top = jnp.max(jnp.maximum(most[0], most[1]), axis=0, keepdims=True)
+        stats[par] = jnp.broadcast_to(top, (8, 256)) * (SCALE * LOG2E)
+
+    def weigh(par, g, count):
+        top = stats[par]
+        for r in range(gz // 16):
+            rows = slice(16 * r, 16 * r + 16)
+            weights = [
+                jnp.exp2(sbufs[par][g, 16 * r + o : 16 * r + o + 8, :] * (SCALE * LOG2E) - top) for o in (0, 8)
+            ]
+            pbufs[par][g, rows, :] = jnp.concatenate(weights, axis=0).astype(BF16)
+            for o in range(2):
+                count[o] = weights[o] if count[o] is None else count[o] + weights[o]
+
+    def weighed(par, count):
+        stats[2 + par] = jnp.broadcast_to(jnp.sum(count[0] + count[1], axis=0, keepdims=True), (8, 256))
+        stats[4 + par] = stats[par] * (1.0 / LOG2E)
+
+    def gather(par, g, accs):
+        update = dot(vtall[g], pbufs[par][g])
+        accs[g % 2] = update if accs[g % 2] is None else accs[g % 2] + update
+
+    def gathered(i, par, accs):
+        yy, _ = ypeer(turn_of(i))
+        acc = accs[0] + accs[1]
+        top, count = stats[4 + par, 0:1, :], stats[2 + par, 0:1, :]
+        log = top + jnp.log(count)
         lsend[yy] = jnp.where(rows_of(8) == 0, log[:, 0:128], log[:, 128:256])
         inv = 1.0 / count
         osend[yy, 0:64, :] = (acc[0:64, 0:128] * inv[:, 0:128]).astype(BF16)
         osend[yy, 64:128, :] = (acc[64:128, 128:256] * inv[:, 128:256]).astype(BF16)
 
-    def step(i, carry):
-        k = lax.rem(jnp.where(lax.rem(i, 2) == 1, (i + 1) // 2, Y - i // 2), Y)
+    def work(i, par, first, second, third):
+        most, count, accs = [None, None], [None, None], [None, None]
+        if first:
+            prepare(i)
+        for g in range(groups):
+            if third:
+                gather(par, g, accs)
+            if first:
+                score(par, g, most)
+            if second:
+                weigh(1 - par, g, count)
+        if third:
+            gathered(i - 2, par, accs)
+        if first:
+            scored(par, most)
+        if second:
+            weighed(1 - par, count)
+
+    def receive(i):
+        k = turn_of(i)
         yy, who = ypeer(k)
         back = lax.rem(Y - k, Y)
-
-        @pl.when(i > 0)
-        def _():
-            remote(qbuf.at[yy], qbuf.at[yy], qy_s.at[back], qy_r.at[back], who).wait_recv()
-
-        attend(yy)
-
-        @pl.when(i > 0)
-        def _():
-            remote(osend.at[yy], orecv.at[y], o_s.at[0, k], o_r.at[0, k], who).start()
-            remote(lsend.at[yy], lrecv.at[y], o_s.at[1, k], o_r.at[1, k], who).start()
-
+        remote(qbuf.at[yy], qbuf.at[yy], qy_s.at[back], qy_r.at[back], who).wait_recv()
+
+    def give(i):
+        k = turn_of(i)
+        yy, who = ypeer(k)
+        remote(osend.at[yy], orecv.at[y], o_s.at[0, k], o_r.at[0, k], who).start()
+        remote(lsend.at[yy], lrecv.at[y], o_s.at[1, k], o_r.at[1, k], who).start()
+
+    receive(jnp.int32(0))
+    work(jnp.int32(0), 0, True, False, False)
+    if Y > 2:
+        receive(jnp.int32(1))
+    work(jnp.int32(1), 1, True, True, False)
+
+    def step(pair, carry):
+        for par in range(2):
+            i = 2 + 2 * pair + par
+
+            @pl.when(i < Y - 1)
+            def _():
+                receive(i)
+
+            work(i, par, True, True, True)
+            give(i - 2)
         return carry
 
-    lax.fori_loop(0, Y, step, 0)
+    lax.fori_loop(0, (Y - 2) // 2, step, 0)
+    work(jnp.int32(Y), 0, False, True, True)
+    give(jnp.int32(Y - 2))
+    work(jnp.int32(Y + 1), 1, False, False, True)
 
     orecv[y] = osend[y]
     lrecv[y] = lsend[y]
@@ -430,14 +505,14 @@
     inputs = [
         tokens, query_down, latent_down, rope_down.T, row(query_latent_gain), row(latent_gain),
         query_up.T, key_up, value_up, row(query_gain), row(key_gain), row(output_gain), output_weight,
-        jnp.asarray(fine), jnp.asarray(coarse), const(query_columns().T), const(rope_spread()),
-        const(sum_matrix(32)), const(sum_matrix(64)), const(gain_columns()),
+        jnp.asarray(fine), jnp.asarray(coarse), const(query_rows()), const(rope_spread()),
+        const(sum_matrix()), const(gain_columns()),
     ]
     return pl.pallas_call(
         functools.partial(kernel, Z, Y, C, X, batches),
         out_shape=(
-            jax.ShapeDtypeStruct((128, output_weight.shape[1]), BF16),
-            jax.ShapeDtypeStruct((2, 128), F32),
+            pltpu.VMEM((128, output_weight.shape[1]), BF16),
+            pltpu.VMEM((2, 128), F32),
         ),
         in_specs=[hbm, sm] + [hbm] * (len(inputs) - 1),
         out_specs=(vm, vm),
@@ -449,6 +524,12 @@
             pltpu.VMEM((groups, gz, 256), BF16),
             pltpu.VMEM((groups, 128, gz), BF16),
             pltpu.VMEM((groups, gz, 256), F32),
+            pltpu.VMEM((groups, gz, 256), F32),
+            pltpu.VMEM((groups, gz, 256), BF16),
+            pltpu.VMEM((groups, gz, 256), BF16),
+            pltpu.VMEM((6, 8, 256), F32),
+            pltpu.VMEM((256, 256), BF16),
+            pltpu.VMEM((256, 128), F32),
             pltpu.VMEM((128, KVR), BF16),
             pltpu.VMEM((Y, 128, 128), BF16),
             pltpu.VMEM((Y, 8, 128), F32),
@@ -456,6 +537,7 @@
             pltpu.VMEM((Y, 8, 128), F32),
             pltpu.VMEM((X, 128, 128), BF16),
             pltpu.VMEM((8, 128), jnp.int32),
+            pltpu.VMEM((2, NDOC, 128), jnp.int32),
             pltpu.VMEM((8, 128), F32),
             dma((len(inputs),)),
             dma((X,)), dma((X,)),
@@ -468,7 +550,7 @@
             dma((X,)), dma((X,)),
         ],
         compiler_params=pltpu.CompilerParams(
-            collective_id=0, has_side_effects=True, vmem_limit_bytes=60 * 2**20
+            collective_id=0, has_side_effects=True, vmem_limit_bytes=56 * 2**20
         ),
     )(tokens, doc_lengths, *inputs[1:])
 

time: 56.7 us -> 49 us (0.86)
  Pallas kernels: 53.1 us -> 47 us
  local copies, waits for them, and re-layouts: 2.8 us -> 1.22 us
    pallas_call x1, Pallas kernels: 53.1 us -> 47 us  [per_device(): pl.pallas_call(functools.partial(kernel, Z, Y, C, X, batches), out_shape=...]
    unnamed x2, local copies, waits for them, and re-layouts: 2.8 us -> 1.22 us
where the time goes in v3:
time: 49 us; the launch traced here: 48.9 us
  Pallas kernels  47 us (96%)
  local copies, waits for them, and re-layouts  1.22 us (2%)
  between operations  0.64 us (1%)
    pallas_call x1, Pallas kernels, per_device(): pl.pallas_call(functools.partial(kernel, Z, Y, C, X, batches), out_shape=...  47 us
    unnamed x2, local copies, waits for them, and re-layouts  1.22 us

profile of v3, /device:TPU:1, one launch (start us, length us, event | category | flops | bytes accessed | tf_op | source)
XLA Modules:
  0.0 48.9 jit_solution(15013388624623312876)
XLA Ops:
  0.6 47.0 %shard_map.203 = (bf16[128,512]{1,0:T(8,128)(2,1)S(1)}, f32[2,128]{1,0:T(2,128)S(1)}) custom-call(bf16[32,2048]{1,0:T(8,128)(2,1)} %tok_h.1, s32[16]{0:T(128)} %doclen.1, bf16[2048,512]{1,0:T(8,128)(2,1)} %qdown_h.1, bf16[2048,256]{1,0:T(8,128)(2,1)} %ldown_h.1, bf16[32,2048]{1,0:T(8,128)(2,1)} %bitcast.8, f32[1,512]{1,0:T(1,128)} %bitcast.9, ...), custom_call_target="tpu_custom_call" | custom-call | tf_op jit(solution)/shard_map/pallas_call | solution.py:511
  47.7 0.7 %copy.24 = bf16[128,512]{1,0:T(8,128)(2,1)} copy(bf16[128,512]{1,0:T(8,128)(2,1)S(1)} %get-tuple-element.2) | data formatting | bytes 262144
  48.3 0.6 %copy.25 = f32[2,128]{1,0:T(2,128)} copy(f32[2,128]{1,0:T(2,128)S(1)} %get-tuple-element.3) | data formatting | bytes 2048
